TPU v7x, 32 devices: a whole 2x2x4 slice. The times are simulated.
32 devices in a mesh: sp: 8 (over z, y), tp: 4 (over x, core).
Axes of the slice: x: 2, y: 2, z: 4, core: 2. Of those that a mesh axis runs over, the one named last changes fastest.
Arguments:
- tokens: bfloat16 [4096, 2048], P(('sp', 'tp')), may hold values from -6 to 6
- queries: bfloat16 [4096, 1024], P('sp', 'tp'), may hold values from -160 to 160
- keys: bfloat16 [4096, 1024], P('sp', 'tp'), may hold values from -8 to 8
- values: bfloat16 [4096, 1024], P('sp', 'tp'), may hold values from -6 to 6
- lambdas: float32 [8], P('tp'), may hold values from 0.3 to 0.8
- head_gain: float32 [128], replicated, may hold values from 0.1 to 1.9
- out_weight: bfloat16 [1024, 2048], replicated, may hold values from -0.1875 to 0.1875
- mixer_gain: float32 [2048], replicated, may hold values from 0.1 to 1.9
- up_weight: bfloat16 [2048, 4096], P('sp', 'tp'), may hold values from -0.125 to 0.125
- down_weight: bfloat16 [4096, 2048], P('tp', 'sp'), may hold values from -0.09375 to 0.09375
Outputs:
- result: bfloat16 [4096, 2048], P(('sp', 'tp'))
All inputs are finite; a program needn't handle non-finite values.
Results may differ from a plain program's by a relative error of at most 0.02.
Values may be sent and summed in bfloat16 or wider, within the bound.
A program may use at most 128 MiB of HBM per device.

v0:
```python
import functools

import jax
import jax.numpy as jnp
from jax import lax
from jax.experimental import pallas as pl
from jax.experimental.pallas import tpu as pltpu
from jax.sharding import PartitionSpec as P

DQK = 64
MESH = pl.DeviceIdType.MESH
f32, bf16 = jnp.float32, jnp.bfloat16


def layer_kernel(
    n, tp,
    lam_ref, q_ref, k_ref, v_ref, gain_ref, up_ref, dn_ref, tok_ref, mix_ref, ow_hbm,
    out_ref,
    ah_ref, upf_ref, dnf_ref,
    qb, kv, qm, run_max, run_sum, acc, att, ow, resid, normed, hsum, hid, part, core_in, cross, cross_in,
    ex_send, ex_recv, kv_send, kv_recv, w_send, own_send, y_send, w_recv, a_send, a_recv, loc,
    ag_send, ag_recv, c_send, c_recv, x_send, x_recv,
):
    s = lax.axis_index("sp")
    t = lax.axis_index("tp")
    z, y = s // 2, lax.rem(s, 2)
    steps = n // 2
    rows = q_ref.shape[0]
    wide = q_ref.shape[1] // 2
    peer = (s + 1 - 2 * y, t)
    above, below = (s + 2, t), (s - 2, t)
    has_up, has_down = z < steps - 1, z > 0
    piece = rows // tp

    barrier = pltpu.get_barrier_semaphore()

    def greet(device):
        pl.semaphore_signal(barrier, inc=1, device_id=device, device_id_type=MESH)

    for e in range(2):
        for i in range(tp):
            who = (2 * z + e, i)

            @pl.when(jnp.logical_or(e != y, i != t))
            def _():
                greet(who)

    pl.when(has_up)(lambda: greet(above))
    pl.when(has_down)(lambda: greet(below))
    pl.semaphore_wait(barrier, 2 * tp - 1 + has_up.astype(jnp.int32) + has_down.astype(jnp.int32))

    def remote(src, dst, send, recv, device):
        return pltpu.make_async_remote_copy(
            src_ref=src, dst_ref=dst, send_sem=send, recv_sem=recv, device_id=device, device_id_type=MESH
        )

    my_rows = pl.ds(pl.multiple_of(y * rows, rows), rows)
    peer_rows = pl.ds(pl.multiple_of((1 - y) * rows, rows), rows)
    my_cols = pl.ds(pl.multiple_of(y * wide, wide), wide)
    peer_cols = pl.ds(pl.multiple_of((1 - y) * wide, wide), wide)
    ex = []
    for i, (src, dst) in enumerate(((k_ref, kv.at[z, 0]), (v_ref, kv.at[z, 1]), (q_ref, qb))):
        ex.append(remote(src.at[:, peer_cols], dst.at[my_rows], ex_send.at[i], ex_recv.at[i], peer))
        ex[-1].start()

    half = dn_ref.shape[0] // 2
    halves = (slice(0, half), slice(half, 2 * half))

    def shard(c, j):
        if c == 0:
            depth = up_ref.shape[0]
            return upf_ref.at[pl.ds(pl.multiple_of(j * depth, depth), depth)]
        return dnf_ref.at[j, halves[c - 1]]

    own = (up_ref, dn_ref.at[halves[0]], dn_ref.at[halves[1]])

    def own_up(c):
        remote(own[c], shard(c, s), w_send.at[s, c], w_recv.at[s, c], above).start()

    pl.when(has_up)(lambda: own_up(0))
    for c in range(3):

        @pl.when(has_down)
        def _():
            remote(own[c], shard(c, s), own_send.at[c], w_recv.at[s, c], below).start()

        remote(own[c], shard(c, s), y_send.at[s, c], w_recv.at[s, c], peer).start()
    local = []
    for i, (src, dst) in enumerate(
        (
            (k_ref.at[:, my_cols], kv.at[z, 0, my_rows]),
            (v_ref.at[:, my_cols], kv.at[z, 1, my_rows]),
            (q_ref.at[:, my_cols], qb.at[my_rows]),
            (up_ref, shard(0, s)),
            (dn_ref, dnf_ref.at[s]),
            (ow_hbm, ow),
        )
    ):
        local.append(pltpu.make_async_copy(src, dst, loc.at[i]))
        local[-1].start()
    for i in range(3):
        local[i].wait()
    for i, (src, dst) in enumerate(((k_ref, kv.at[z, 0]), (v_ref, kv.at[z, 1]), (q_ref, qb))):
        remote(src.at[:, peer_cols], dst.at[peer_rows], ex_send.at[i], ex_recv.at[i], peer).wait_recv()

    def onward(c, j, device):
        moved = shard(c, j)
        remote(moved, moved, w_send.at[j, c], w_recv.at[j, c], device).start()

    def await_chunk(c, j):
        moved = shard(c, j)
        remote(moved, moved, w_send.at[j, c], w_recv.at[j, c], peer).wait_recv()

    def over(c, j):
        moved = shard(c, j)
        remote(moved, moved, y_send.at[j, c], w_recv.at[j, c], peer).start()

    def arrive(c, j, device, exists):
        await_chunk(c, j)
        over(c, j)
        pl.when(exists)(lambda: onward(c, j, device))

    def next_above(c):
        @pl.when(z + 1 < steps)
        def _():
            await_chunk(c, s + 2)
            pl.when(has_down)(lambda: onward(c, s + 2, below))

    def down_up():
        own_up(1)
        own_up(2)

    def from_above(d):
        for c in range(3):
            pl.when(z + d < steps)(lambda: arrive(c, s + 2 * d, below, has_down))

    def kv_forward(j):
        return remote(kv.at[j], kv.at[j], kv_send.at[j], kv_recv.at[j], above)

    @pl.when(has_up)
    def _():
        kv_forward(z).start()
        pl.when(jnp.logical_or(z == 0, z == steps - 2))(down_up)

    total = 2 * rows
    lane = lax.broadcasted_iota(jnp.int32, (total, wide), 1)
    scaled = qb[...] * jnp.asarray(DQK ** -0.5, bf16)
    for m in range(2):
        qm[m * total:(m + 1) * total, :] = jnp.where((lane < DQK) == (m == 0), scaled, jnp.zeros_like(scaled))

    chunk = min(256, total)

    def scores_of(r0, j, keys):
        return lax.dot_general(
            qm[pl.ds(r0, chunk), :], kv[j, 0, :keys, :], (((1,), (1,)), ((), ())), preferred_element_type=f32
        )

    for m in range(2):
        for b in range(total // chunk):
            r0, keys = m * total + b * chunk, (b + 1) * chunk
            sc = scores_of(r0, z, keys)
            qpos = b * chunk + lax.broadcasted_iota(jnp.int32, (chunk, keys), 0)
            kpos = lax.broadcasted_iota(jnp.int32, (chunk, keys), 1)
            sc = jnp.where(kpos <= qpos, sc, -jnp.inf)
            top = jnp.max(sc, axis=1, keepdims=True)
            p = jnp.exp(sc - top)
            run_max[pl.ds(r0, chunk), :] = jnp.broadcast_to(top, (chunk, 128))
            run_sum[pl.ds(r0, chunk), :] = jnp.broadcast_to(jnp.sum(p, axis=1, keepdims=True), (chunk, 128))
            acc[pl.ds(r0, chunk), :] = jnp.dot(p.astype(bf16), kv[z, 1, :keys, :], preferred_element_type=f32)

    def block(d, carry):
        j = z - d
        @pl.when(d == 1)
        def _():
            await_chunk(0, s - 2)
            over(0, s - 2)
            next_above(0)

        @pl.when(jnp.logical_and(d == 2, z == steps - 1))
        def _():
            for c in (1, 2):
                await_chunk(c, s - 2)
                over(c, s - 2)

        kv_forward(j).wait_recv()

        @pl.when(has_up)
        def _():
            kv_forward(j).start()

            @pl.when(j == 0)
            def _():
                onward(0, s - 2, above)
                if steps != 3:
                    pl.when(z == 1)(down_up)

        @pl.when(d == 1)
        def _():
            next_above(1)
            next_above(2)

        def tile(b, inner):
            r0 = pl.multiple_of(b * chunk, chunk)
            here = pl.ds(r0, chunk)
            sc = scores_of(r0, j, total)
            old = run_max[here, :]
            top = jnp.maximum(old, jnp.max(sc, axis=1, keepdims=True))
            p = jnp.exp(sc - top[:, :1])
            shrink = jnp.exp(old - top)
            run_max[here, :] = top
            run_sum[here, :] = run_sum[here, :] * shrink + jnp.sum(p, axis=1, keepdims=True)
            acc[here, :] = acc[here, :] * shrink + jnp.dot(p.astype(bf16), kv[j, 1], preferred_element_type=f32)
            return inner

        lax.fori_loop(0, 2 * total // chunk, tile, 0)
        return carry

    lax.fori_loop(1, z + 1, block, 0)

    lam = lam_ref[y]
    differ = acc[:total, :] / run_sum[:total, :] - lam * (acc[total:, :] / run_sum[total:, :])
    spread = lax.rsqrt(jnp.mean(differ * differ, axis=1, keepdims=True) + 1e-06)
    att[...] = (differ * spread * gain_ref[...]).astype(bf16)

    head = 2 * t + y
    head_cols = pl.ds(pl.multiple_of(head * wide, wide), wide)

    def to_token(e, i, head_index):
        cols = pl.ds(pl.multiple_of(head_index * wide, wide), wide)
        return remote(
            att.at[pl.ds(e * rows + i * piece, piece)], ah_ref.at[:, cols],
            a_send.at[e * tp + i], a_recv.at[head_index], (2 * z + e, i),
        )

    mine = pltpu.make_async_copy(
        att.at[pl.ds(pl.multiple_of(y * rows + t * piece, piece), piece)], ah_ref.at[:, head_cols], loc.at[6]
    )
    mine.start()
    for e in range(2):
        for i in range(tp):
            pl.when(jnp.logical_or(e != y, i != t))(lambda: to_token(e, i, head).start())

    def up_below(d):
        @pl.when(z - d >= 0)
        def _():
            arrive(0, s - 2 * d, above, has_up)
            pl.when(jnp.logical_and(d == z, z < steps - 2))(down_up)

    @pl.when(z == 0)
    def _():
        for c in range(3):
            next_above(c)

    @pl.when(z + 1 < steps)
    def _():
        for c in range(3):
            over(c, s + 2)

    up_below(2)
    local[5].wait()
    mine.wait()
    for i in range(2 * tp):
        e, who = i % 2, i // 2
        pl.when(jnp.logical_or(e != y, who != t))(lambda: to_token(0, 0, i).wait_recv())

    projected = jnp.dot(ah_ref[...], ow[...], preferred_element_type=f32).astype(bf16)
    summed = (tok_ref[...].astype(f32) + projected.astype(f32)).astype(bf16)
    resid[...] = summed
    summed = summed.astype(f32)
    scale = lax.rsqrt(jnp.mean(summed * summed, axis=1, keepdims=True) + 1e-06)

    tc = t + 1 - 2 * lax.rem(t, 2)
    tx = lax.rem(t + 2, tp)
    td = lax.rem(tc + 2, tp)

    def band(i):
        return pl.ds(pl.multiple_of(i * piece, piece), piece)

    normed[band(t), :] = (summed * scale * mix_ref[...]).astype(bf16)

    def gathered(k, block_index, device):
        block_ref = normed.at[band(block_index)]
        return remote(block_ref, block_ref, ag_send.at[k], ag_recv.at[block_index], (s, device))

    gathered(0, t, tx).start()
    gathered(1, t, tc).start()

    def pump(d, carry):
        pl.when(d > 2)(lambda: up_below(d))
        from_above(d)
        return carry

    lax.fori_loop(2, min(3, steps), pump, 0)
    gathered(0, tx, tx).wait_recv()
    gathered(2, tx, tc).start()
    lax.fori_loop(min(3, steps), steps, pump, 0)
    gathered(1, tc, tc).wait_recv()
    gathered(2, td, tc).wait_recv()
    local[3].wait()
    local[4].wait()

    def order(k):
        return jnp.where(k < steps - z, z + k, steps - 1 - k)

    def across(c, i):
        j = 2 * i + 1 - y
        remote(shard(c, j), shard(c, j), y_send.at[j, c], w_recv.at[j, c], peer).wait_recv()

    def down_below(i):
        @pl.when(jnp.logical_and(i >= 0, i < z))
        def _():
            arrive(1, 2 * i + y, above, has_up)
            arrive(2, 2 * i + y, above, has_up)

    pl.when(jnp.logical_or(z < steps - 1, z < 2))(lambda: down_below(z - 1))
    pair_depth = 2 * up_ref.shape[0]
    hsum[...] = jnp.zeros_like(hsum)

    def up_pair(k, carry):
        i = order(k)
        across(0, i)
        span = pl.ds(pl.multiple_of(i * pair_depth, pair_depth), pair_depth)
        hsum[...] += jnp.dot(normed[:, span], upf_ref[span, :], preferred_element_type=f32)
        return carry

    lax.fori_loop(0, steps, up_pair, 0)
    hid[...] = jnp.square(jnp.maximum(hsum[...], 0.0)).astype(bf16)

    def to_core(j, m):
        return remote(
            part.at[j, band(tc if m == 0 else td)], core_in.at[j, m], c_send.at[j, m], c_recv.at[j, m], (s, tc)
        )

    def to_cross(j):
        return remote(cross.at[j], cross_in.at[j], x_send.at[j], x_recv.at[j], (s, tx))

    def add_cores(i):
        for e in range(2):
            j = 2 * i + e
            to_core(j, 1).wait_recv()
            cross[j] = (part[j, band(tx), :].astype(f32) + core_in[j, 1].astype(f32)).astype(bf16)
            to_cross(j).start()

    def down_pair(k, carry):
        i = order(k)
        later = order(k + 1)

        pl.when(jnp.logical_and(k + 1 < steps, later < z - 1))(lambda: down_below(later))
        pl.when(k > 0)(lambda: add_cores(order(k - 1)))
        across(1, i)
        across(2, i)
        for e in range(2):
            j = 2 * i + e
            part[j] = jnp.dot(hid[...], dnf_ref[j], preferred_element_type=f32).astype(bf16)
            to_core(j, 1).start()
            to_core(j, 0).start()
        return carry

    lax.fori_loop(0, steps, down_pair, 0)
    add_cores(order(steps - 1))

    cols = dn_ref.shape[1]
    for j in range(n):
        to_core(j, 0).wait_recv()
        to_cross(j).wait_recv()
        here = slice(j * cols, (j + 1) * cols)
        both = part[j, band(t), :].astype(f32) + core_in[j, 0].astype(f32) + cross_in[j].astype(f32)
        out_ref[:, here] = (resid[:, here].astype(f32) + both).astype(bf16)

    gathered(0, t, tx).wait_send()
    gathered(1, t, tc).wait_send()
    gathered(2, tx, tc).wait_send()
    for j in range(n):
        to_core(j, 0).wait_send()
        to_core(j, 1).wait_send()
        to_cross(j).wait_send()
    for copy in ex:
        copy.wait_send()
    for e in range(2):
        for i in range(tp):
            pl.when(jnp.logical_or(e != y, i != t))(lambda: to_token(e, i, head).wait_send())

    @pl.when(has_up)
    def _():
        def sent(j, carry):
            kv_forward(j).wait_send()
            return carry

        lax.fori_loop(0, z + 1, sent, 0)

    def line_sent(i, carry):
        j = 2 * i + y
        for c in range(3):
            moved = shard(c, j)
            remote(moved, moved, y_send.at[j, c], w_recv.at[j, c], peer).wait_send()
            gone = jnp.logical_or(jnp.logical_and(i <= z, has_up), jnp.logical_and(i > z, has_down))
            pl.when(gone)(lambda: remote(moved, moved, w_send.at[j, c], w_recv.at[j, c], peer).wait_send())
        return carry

    lax.fori_loop(0, steps, line_sent, 0)

    @pl.when(has_down)
    def _():
        for c in range(3):
            remote(own[c], shard(c, s), own_send.at[c], w_recv.at[s, c], below).wait_send()


def per_device(
    n, tp, tokens, queries, keys, values, lambdas, head_gain, out_weight, mixer_gain, up_weight, down_weight
):
    rows, wide = queries.shape[0], queries.shape[1] // 2
    depth, units = up_weight.shape
    cols = down_weight.shape[1]
    piece, width = tokens.shape
    vmem = pl.BlockSpec(memory_space=pltpu.VMEM)
    dma = pltpu.SemaphoreType.DMA
    return pl.pallas_call(
        functools.partial(layer_kernel, n, tp),
        out_shape=jax.ShapeDtypeStruct(tokens.shape, bf16),
        in_specs=[pl.BlockSpec(memory_space=pltpu.SMEM)] + [vmem] * 8 + [pl.BlockSpec(memory_space=pl.ANY)],
        out_specs=vmem,
        scratch_shapes=[
            pltpu.VMEM((piece, 2 * tp * wide), bf16),
            pltpu.VMEM((n * depth, units), bf16),
            pltpu.VMEM((n, units, cols), bf16),
            pltpu.VMEM((2 * rows, wide), bf16),
            pltpu.VMEM((n // 2, 2, 2 * rows, wide), bf16),
            pltpu.VMEM((4 * rows, wide), bf16),
            pltpu.VMEM((4 * rows, 128), f32),
            pltpu.VMEM((4 * rows, 128), f32),
            pltpu.VMEM((4 * rows, wide), f32),
            pltpu.VMEM((2 * rows, wide), bf16),
            pltpu.VMEM(out_weight.shape, bf16),
            pltpu.VMEM((piece, width), bf16),
            pltpu.VMEM((rows, width), bf16),
            pltpu.VMEM((rows, units), f32),
            pltpu.VMEM((rows, units), bf16),
            pltpu.VMEM((n, rows, cols), bf16),
            pltpu.VMEM((n, 2, piece, cols), bf16),
            pltpu.VMEM((n, piece, cols), bf16),
            pltpu.VMEM((n, piece, cols), bf16),
            dma((3,)), dma((3,)), dma((n // 2,)), dma((n // 2,)),
            dma((n, 3)), dma((3,)), dma((n, 3)), dma((n, 3)), dma((2 * tp,)), dma((2 * tp,)), dma((7,)),
            dma((3,)), dma((tp,)), dma((n, 2)), dma((n, 2)), dma((n,)), dma((n,)),
        ],
        compiler_params=pltpu.CompilerParams(
            collective_id=0, has_side_effects=True, vmem_limit_bytes=60 * 1024 * 1024
        ),
    )(
        lambdas, queries, keys, values, head_gain.reshape(1, -1), up_weight, down_weight,
        tokens, mixer_gain.reshape(1, -1), out_weight,
    )


def solution(mesh):
    placed = (
        P(("sp", "tp"), None),
        P("sp", "tp"),
        P("sp", "tp"),
        P("sp", "tp"),
        P("tp"),
        P(),
        P(),
        P(),
        P("sp", "tp"),
        P("tp", "sp"),
    )
    return jax.shard_map(
        functools.partial(per_device, mesh.shape["sp"], mesh.shape["tp"]),
        mesh=mesh,
        in_specs=placed,
        out_specs=P(("sp", "tp"), None),
        check_vma=False,
    )
```

profile of v0, /device:TPU:25, one launch (start us, length us, event | category | flops | bytes accessed | tf_op | source)
XLA Modules:
  0.0 134.2 jit_solution(9213179019359941029)
XLA Ops:
  0.0 132.3 %shard_map.100 = bf16[128,2048]{1,0:T(8,128)(2,1)} custom-call(f32[2]{0:T(128)} %lam_ref.1, bf16[512,256]{1,0:T(8,128)(2,1)} %q_ref.1, bf16[512,256]{1,0:T(8,128)(2,1)} %k_ref.1, bf16[512,256]{1,0:T(8,128)(2,1)} %v_ref.1, f32[1,128]{1,0:T(1,128)} %bitcast.3, bf16[256,1024]{1,0:T(8,128)(2,1)} %up_ref.1, bf16[1024,256]{1,0:T(8,128)(2,1)} %dn_ref.1, ...), custom_call_target="tpu_custom_call" | custom-call | tf_op jit(solution)/shard_map/pallas_call | solution.py:417
  132.3 1.9 %copy.12 = bf16[128,2048]{1,0:T(8,128)(2,1)} copy(bf16[128,2048]{1,0:T(8,128)(2,1)} %shard_map.100) | data formatting | bytes 1048576
where the time goes:
time: 136 us; the launch traced here: 134 us
  Pallas kernels  132 us (97%)
  local copies, waits for them, and re-layouts  1.88 us (1%)
    pallas_call x1, Pallas kernels, per_device(): pl.pallas_call(functools.partial(layer_kernel, n, tp), out_shape=jax.Shap...  132 us

commit v1 on v0

v1 whole, which is shorter than its diff:
```python
import functools

import jax
import jax.numpy as jnp
from jax import lax
from jax.experimental import pallas as pl
from jax.experimental.pallas import tpu as pltpu
from jax.sharding import PartitionSpec as P

DQK = 64
MESH = pl.DeviceIdType.MESH
f32, bf16 = jnp.float32, jnp.bfloat16
CHUNKS = 4
UPS, DOWNS = (0, 1), (2, 3)


def layer_kernel(
    n, tp,
    lam_ref, q_ref, k_ref, v_ref, gain_ref, up_ref, dn_ref, tok_ref, mix_ref, ow_hbm,
    out_ref,
    ah, upf_ref, dnf_ref,
    qb, kv, qm, run_max, run_sum, acc, att, att_above, ow, tokall, normed, hsum, hid, part, core_in, cross, cross_in,
    ex_send, ex_recv, top_recv, swap_send, tk_send, tk_recv, kv_send, kv_recv,
    w_send, own_send, y_send, w_recv, u_send, u_recv, a_send, a_recv, loc,
    c_send, c_recv, x_send, x_recv,
):
    s = lax.axis_index("sp")
    t = lax.axis_index("tp")
    z, y = s // 2, lax.rem(s, 2)
    x, c = t // 2, lax.rem(t, 2)
    steps = n // 2
    rows = q_ref.shape[0]
    wide = q_ref.shape[1] // 2
    total = 2 * rows
    piece = rows // tp
    top, helper = z == steps - 1, z == steps - 2
    has_up, has_down = z < steps - 1, z > 0
    above, below = (s + 2, t), (s - 2, t)
    beside = (s + 1 - 2 * y, t)
    core = (s, t + 1 - 2 * c)
    across_x = (s, lax.rem(t + 2, tp))
    corner = (s + 1 - 2 * y, lax.rem(t + 2, tp))
    line = 2 * z + c
    own_line = y == c
    partner = (line, 2 * x + y)

    barrier = pltpu.get_barrier_semaphore()

    def greet(device):
        pl.semaphore_signal(barrier, inc=1, device_id=device, device_id_type=MESH)

    for e in range(2):
        for i in range(tp):
            who = (2 * z + e, i)

            @pl.when(jnp.logical_or(e != y, i != t))
            def _():
                greet(who)

    pl.when(has_up)(lambda: greet(above))
    pl.when(has_down)(lambda: greet(below))
    pl.when(top)(lambda: greet((s - 2 + 1 - 2 * y, t)))
    pl.when(helper)(lambda: greet((s + 2 + 1 - 2 * y, t)))
    pl.semaphore_wait(
        barrier,
        2 * tp - 1 + has_up.astype(jnp.int32) + has_down.astype(jnp.int32)
        + jnp.logical_or(top, helper).astype(jnp.int32),
    )

    def remote(src, dst, send, recv, device):
        return pltpu.make_async_remote_copy(
            src_ref=src, dst_ref=dst, send_sem=send, recv_sem=recv, device_id=device, device_id_type=MESH
        )

    def rows_of(e):
        return pl.ds(pl.multiple_of(e * rows, rows), rows)

    def cols_of(e):
        return pl.ds(pl.multiple_of(e * wide, wide), wide)

    my_rows, peer_rows = rows_of(y), rows_of(1 - y)
    my_cols, peer_cols = cols_of(y), cols_of(1 - y)
    qkv = (q_ref, k_ref, v_ref)

    def landing(i, plane, slot, where):
        return qb.at[slot, where] if i == 0 else kv.at[plane, i - 1, where]

    def exchange(i, where):
        return remote(
            qkv[i].at[:, peer_cols], landing(i, z, 0, where), ex_send.at[0, i], ex_recv.at[i], beside
        )

    def lower(i, e):
        cols = my_cols if e == 0 else peer_cols
        device = below if e == 0 else (s - 2 + 1 - 2 * y, t)
        return remote(
            qkv[i].at[:, cols], landing(i, z, 1, my_rows), ex_send.at[e, i], top_recv.at[y, i], device
        )

    @pl.when(jnp.logical_not(top))
    def _():
        for i in (1, 2, 0):
            exchange(i, my_rows).start()

    @pl.when(top)
    def _():
        for i in range(3):
            for e in range(2):
                lower(i, e).start()

    depth, units = up_ref.shape
    half_depth, half = depth // 2, units // 2

    def shard(k, j):
        if k in UPS:
            return upf_ref.at[pl.ds(pl.multiple_of(j * depth + k * half_depth, half_depth), half_depth)]
        return dnf_ref.at[j, slice((k - 2) * half, (k - 1) * half)]

    given = (
        up_ref.at[slice(0, half_depth)], up_ref.at[slice(half_depth, depth)],
        dn_ref.at[slice(0, half)], dn_ref.at[slice(half, units)],
    )

    def swap(k):
        return remote(given[k], shard(k, s), swap_send.at[k], w_recv.at[s, k], partner)

    def send_above(k, j, src):
        remote(src, shard(k, j), w_send.at[j, k], w_recv.at[j, k], above).start()

    def send_below(k, j, src, sems):
        remote(src, shard(k, j), sems, w_recv.at[j, k], below).start()

    def over(k, j, src):
        remote(src, shard(k, j), y_send.at[j, k], w_recv.at[j, k], core).start()

    early_down = jnp.logical_or(z == 0, helper)

    def own_above(k, src):
        pl.when(has_up)(lambda: send_above(k, line, src))

    def own_around(k, src):
        pl.when(has_down)(lambda: send_below(k, line, src, own_send.at[k]))
        over(k, line, src)

    @pl.when(own_line)
    def _():
        for k in UPS:
            own_above(k, given[k])
        for k in UPS + DOWNS:
            own_around(k, given[k])

    @pl.when(jnp.logical_not(own_line))
    def _():
        for k in UPS + DOWNS:
            swap(k).start()

    def band(i):
        return pl.ds(pl.multiple_of(i * piece, piece), piece)

    b = 2 * y + x
    bx = b + 1 - 2 * x
    by = lax.rem(b + 2, tp)
    bd = lax.rem(bx + 2, tp)

    def token_copy(k, source, device):
        return remote(tok_ref, tokall.at[band(source)], tk_send.at[k], tk_recv.at[source], device)

    token_copy(0, b, across_x).start()

    def local_copy(i):
        src, dst = (
            (k_ref.at[:, my_cols], kv.at[z, 0, my_rows]),
            (v_ref.at[:, my_cols], kv.at[z, 1, my_rows]),
            (q_ref.at[:, my_cols], qb.at[0, my_rows]),
            (up_ref, upf_ref.at[pl.ds(pl.multiple_of(s * depth, depth), depth)]),
            (dn_ref, dnf_ref.at[s]),
            (ow_hbm, ow),
            (tok_ref, tokall.at[band(b)]),
        )[i]
        return pltpu.make_async_copy(src, dst, loc.at[i])

    @pl.when(jnp.logical_not(top))
    def _():
        for i in range(3):
            local_copy(i).start()

    @pl.when(own_line)
    def _():
        local_copy(3).start()
        local_copy(4).start()

    local_copy(5).start()
    local_copy(6).start()

    def kv_up(j):
        return remote(kv.at[j], kv.at[j], kv_send.at[j], kv_recv.at[j], above)

    kv_rises = z < steps - 2

    @pl.when(jnp.logical_not(top))
    def _():
        for i in range(3):
            local_copy(i).wait()
        for i in (1, 2, 0):
            exchange(i, peer_rows).wait_recv()
        pl.when(kv_rises)(lambda: kv_up(z).start())

    @pl.when(jnp.logical_and(own_line, early_down))
    def _():
        for k in DOWNS:
            own_above(k, given[k])

    def await_chunk(k, j):
        moved = shard(k, j)
        remote(moved, moved, w_send.at[j, k], w_recv.at[j, k], core).wait_recv()

    def swapped(ks):
        @pl.when(jnp.logical_not(own_line))
        def _():
            for k in ks:
                await_chunk(k, line)
                src = shard(k, line)
                if k in UPS:
                    own_above(k, src)
                else:
                    pl.when(early_down)(lambda: own_above(k, src))
                own_around(k, src)

    def late_down():
        @pl.when(own_line)
        def _():
            for k in DOWNS:
                own_above(k, given[k])

        @pl.when(jnp.logical_not(own_line))
        def _():
            for k in DOWNS:
                own_above(k, shard(k, line))

    def from_above(d, ks):
        j = line + 2 * d
        for k in ks:
            await_chunk(k, j)
            src = shard(k, j)
            pl.when(has_down)(lambda: send_below(k, j, src, w_send.at[j, k]))
            over(k, j, src)

    def from_below(d, ks):
        j = line - 2 * d
        for k in ks:
            await_chunk(k, j)
            src = shard(k, j)
            pl.when(has_up)(lambda: send_above(k, j, src))
            over(k, j, src)

    chunk = min(512, total)
    lane = lax.broadcasted_iota(jnp.int32, (total, wide), 1)

    def weigh(sc, top_row):
        parts, whole = [], None
        for i in range(sc.shape[1] // 128):
            p = jnp.exp(sc[:, i * 128:(i + 1) * 128] - top_row)
            whole = p if whole is None else whole + p
            parts.append(p.astype(bf16))
        return jnp.concatenate(parts, axis=1), whole

    def scores_of(u, r0, j, keys):
        return lax.dot_general(
            qm[u, pl.ds(r0, chunk), :], kv[j, 0, :keys, :], (((1,), (1,)), ((), ())), preferred_element_type=f32
        )

    def diagonal(u, carry):
        @pl.when(u == 1)
        def _():
            for e in range(2):
                for i in range(3):
                    dst = landing(i, z + 1, 1, rows_of(e))
                    remote(dst, dst, ex_send.at[0, i], top_recv.at[e, i], above).wait_recv()

        scaled = qb[u] * jnp.asarray(DQK ** -0.5, bf16)
        for m in range(2):
            qm[u, m * total:(m + 1) * total, :] = jnp.where((lane < DQK) == (m == 0), scaled, jnp.zeros_like(scaled))
        j = z + u
        for m in range(2):
            for i in range(total // chunk):
                r0, keys = m * total + i * chunk, (i + 1) * chunk
                here = pl.ds(r0, chunk)
                sc = scores_of(u, r0, j, keys)
                qpos = i * chunk + lax.broadcasted_iota(jnp.int32, (chunk, keys), 0)
                kpos = lax.broadcasted_iota(jnp.int32, (chunk, keys), 1)
                sc = jnp.where(kpos <= qpos, sc, -jnp.inf)
                top_row = jnp.broadcast_to(jnp.max(sc, axis=1, keepdims=True), (chunk, 128))
                p, whole = weigh(sc, top_row)
                run_max[u, here, :] = top_row
                run_sum[u, here, :] = whole
                acc[u, here, :] = jnp.dot(p, kv[j, 1, :keys, :], preferred_element_type=f32)
        return carry

    def tiles(u, j):
        def tile(i, carry):
            r0 = pl.multiple_of(i * chunk, chunk)
            here = pl.ds(r0, chunk)
            sc = scores_of(u, r0, j, total)
            old = run_max[u, here, :]
            top_row = jnp.maximum(old, jnp.max(sc, axis=1, keepdims=True))
            p, whole = weigh(sc, top_row)
            shrink = jnp.exp(old - top_row)
            run_max[u, here, :] = top_row
            run_sum[u, here, :] = run_sum[u, here, :] * shrink + whole
            acc[u, here, :] = acc[u, here, :] * shrink + jnp.dot(p, kv[j, 1], preferred_element_type=f32)
            return carry

        lax.fori_loop(0, 2 * total // chunk, tile, 0)

    def finish(u, dst):
        lam = lam_ref[y]
        maps = []
        for m in range(2):
            here = slice(m * total, (m + 1) * total)
            maps.append(acc[u, here, :] / jnp.sum(run_sum[u, here, :], axis=1, keepdims=True))
        differ = maps[0] - lam * maps[1]
        spread = lax.rsqrt(jnp.mean(differ * differ, axis=1, keepdims=True) + 1e-06)
        dst[...] = (differ * spread * gain_ref[...]).astype(bf16).reshape(dst.shape)

    def raise_att():
        return remote(att_above, att, u_send.at[0], u_recv.at[0], above)

    @pl.when(jnp.logical_not(top))
    def _():
        diagonal(0, 0)

    swapped(UPS)

    @pl.when(helper)
    def _():
        lax.fori_loop(1, 2, diagonal, 0)
        tiles(1, z)

    swapped(DOWNS)
    token_copy(1, b, beside).start()
    token_copy(2, b, corner).start()

    def block(d, carry):
        j = z - d
        kv_up(j).wait_recv()
        pl.when(kv_rises)(lambda: kv_up(j).start())

        def slot(v, inner):
            u = 1 - v

            @pl.when(jnp.logical_and(u == 0, d == 2))
            def _():
                from_below(1, UPS)

            tiles(u, j)

            @pl.when(jnp.logical_and(u == 1, d == z))
            def _():
                finish(1, att_above)
                raise_att().start()

            return inner

        lax.fori_loop(jnp.where(helper, 0, 1), 2, slot, 0)
        pl.when(d == 1)(lambda: from_above(1, UPS))
        pl.when(d == 2)(lambda: from_above(1, DOWNS))
        return carry

    lax.fori_loop(1, jnp.where(top, 1, z + 1), block, 0)
    pl.when(jnp.logical_not(top))(lambda: finish(0, att))

    @pl.when(top)
    def _():
        from_below(1, UPS + DOWNS)
        from_below(2, UPS)
        raise_att().wait_recv()

    head = 2 * t + y

    def head_cols(i):
        return pl.ds(pl.multiple_of(i * wide, wide), wide)

    def to_tokens(e, i, owner):
        return remote(
            att.at[:, i % 2], ah.at[:, :, head_cols(owner)], a_send.at[e * tp + i], a_recv.at[owner], (2 * z + e, i)
        )

    mine = pltpu.make_async_copy(att.at[:, c], ah.at[:, :, head_cols(head)], loc.at[7])
    mine.start()
    for e in range(2):
        for i in range(tp):
            pl.when(jnp.logical_or(e != y, i != t))(lambda: to_tokens(e, i, head).start())

    @pl.when(z == 0)
    def _():
        from_above(1, UPS + DOWNS)

    @pl.when(z == 1)
    def _():
        from_above(1, DOWNS)
        from_below(1, UPS)
        late_down()

    @pl.when(jnp.logical_and(z >= 2, has_up))
    def _():
        from_below(2, UPS)

    @pl.when(top)
    def _():
        from_below(3, UPS)

    local_copy(5).wait()
    local_copy(6).wait()
    mine.wait()
    for k, (source, device) in enumerate(((bx, across_x), (by, beside), (bd, corner))):
        token_copy(k, source, device).wait_recv()
    for i in range(2 * tp):
        e, who = i % 2, i // 2
        pl.when(jnp.logical_or(e != y, who != t))(lambda: to_tokens(0, 0, i).wait_recv())

    def project(i, carry):
        span = pl.ds(pl.multiple_of(2 * i * piece, 2 * piece), 2 * piece)
        heads = ah[pl.ds(2 * i, 2)].reshape(2 * piece, 2 * tp * wide)
        projected = jnp.dot(heads, ow[...], preferred_element_type=f32).astype(bf16)
        summed = (tokall[span, :].astype(f32) + projected.astype(f32)).astype(bf16)
        tokall[span, :] = summed
        summed = summed.astype(f32)
        scale = lax.rsqrt(jnp.mean(summed * summed, axis=1, keepdims=True) + 1e-06)
        normed[span, :] = (summed * scale * mix_ref[...]).astype(bf16)
        return carry

    lax.fori_loop(0, tp // 2, project, 0)

    def later_ups(d, carry):
        pl.when(z + d < steps)(lambda: from_above(d, UPS))
        waits = jnp.logical_and(d >= 3, jnp.logical_not(jnp.logical_and(top, d == 3)))
        pl.when(jnp.logical_and(z - d >= 0, waits))(lambda: from_below(d, UPS))
        return carry

    lax.fori_loop(2, steps, later_ups, 0)
    pl.when(jnp.logical_and(z > 1, kv_rises))(late_down)
    pl.when(jnp.logical_and(z >= 1, has_up))(lambda: from_below(1, DOWNS))

    @pl.when(own_line)
    def _():
        local_copy(3).wait()
        local_copy(4).wait()

    def order(k):
        return jnp.where(k < steps - z, z + k, steps - 1 - k)

    def from_core(k, i):
        await_chunk(k, 2 * i + 1 - c)

    pair_depth = 2 * depth
    hsum[...] = jnp.zeros_like(hsum)

    def up_pair(k, carry):
        i = order(k)
        for m in UPS:
            from_core(m, i)
        span = pl.ds(pl.multiple_of(i * pair_depth, pair_depth), pair_depth)
        hsum[...] += jnp.dot(normed[:, span], upf_ref[span, :], preferred_element_type=f32)
        return carry

    lax.fori_loop(0, steps, up_pair, 0)
    hid[...] = jnp.square(jnp.maximum(hsum[...], 0.0)).astype(bf16)

    first = ((across_x, bx), (beside, by))

    def to_first(j, e, m):
        device, where = first[e]
        return remote(
            part.at[j, band(where if m == 0 else bd)], core_in.at[j, m], c_send.at[j, m], c_recv.at[j, m], device
        )

    def to_second(j, e):
        return remote(cross.at[j], cross_in.at[j], x_send.at[j], x_recv.at[j], first[1 - e][0])

    def relay(i):
        for e in range(2):
            j = 2 * i + e
            to_first(j, e, 1).wait_recv()
            where = first[1 - e][1]
            cross[j] = (part[j, band(where), :].astype(f32) + core_in[j, 1].astype(f32)).astype(bf16)
            to_second(j, e).start()

    def down_pair(k, carry):
        i = order(k)
        last = k == steps - 1
        pl.when(last)(lambda: relay(order(k - 1)))
        pl.when(i - z >= 2)(lambda: from_above(i - z, DOWNS))
        pl.when(z - i >= 2)(lambda: from_below(z - i, DOWNS))
        for m in DOWNS:
            from_core(m, i)
        for e in range(2):
            j = 2 * i + e
            part[j] = jnp.dot(hid[...], dnf_ref[j], preferred_element_type=f32).astype(bf16)
            to_first(j, e, 1).start()
            to_first(j, e, 0).start()
        pl.when(jnp.logical_and(k > 0, k < steps - 1))(lambda: relay(order(k - 1)))
        return carry

    lax.fori_loop(0, steps, down_pair, 0)
    relay(order(steps - 1))

    cols = dn_ref.shape[1]
    for j in reversed(range(n)):
        to_first(j, j % 2, 0).wait_recv()
        to_second(j, j % 2).wait_recv()
        here = slice(j * cols, (j + 1) * cols)
        both = part[j, band(b), :].astype(f32) + core_in[j, 0].astype(f32) + cross_in[j].astype(f32)
        out_ref[:, here] = (tokall[band(b), here].astype(f32) + both).astype(bf16)

    for j in range(n):
        to_first(j, j % 2, 0).wait_send()
        to_first(j, j % 2, 1).wait_send()
        to_second(j, j % 2).wait_send()
    for k, device in enumerate((across_x, beside, corner)):
        token_copy(k, b, device).wait_send()
    for e in range(2):
        for i in range(tp):
            pl.when(jnp.logical_or(e != y, i != t))(lambda: to_tokens(e, i, head).wait_send())

    @pl.when(jnp.logical_not(top))
    def _():
        for i in range(3):
            exchange(i, my_rows).wait_send()

    @pl.when(top)
    def _():
        for i in range(3):
            for e in range(2):
                lower(i, e).wait_send()

    @pl.when(jnp.logical_not(own_line))
    def _():
        for k in UPS + DOWNS:
            swap(k).wait_send()

    pl.when(helper)(lambda: raise_att().wait_send())

    @pl.when(kv_rises)
    def _():
        def sent(j, carry):
            kv_up(j).wait_send()
            return carry

        lax.fori_loop(0, z + 1, sent, 0)

    def line_sent(i, carry):
        j = 2 * i + c
        for k in UPS + DOWNS:
            moved = shard(k, j)
            remote(moved, moved, y_send.at[j, k], w_recv.at[j, k], core).wait_send()
            gone = jnp.logical_or(jnp.logical_and(i <= z, has_up), jnp.logical_and(i > z, has_down))
            pl.when(gone)(lambda: remote(moved, moved, w_send.at[j, k], w_recv.at[j, k], core).wait_send())
        return carry

    lax.fori_loop(0, steps, line_sent, 0)

    @pl.when(has_down)
    def _():
        for k in UPS + DOWNS:
            moved = shard(k, line)
            remote(moved, moved, own_send.at[k], w_recv.at[line, k], core).wait_send()


def per_device(
    n, tp, tokens, queries, keys, values, lambdas, head_gain, out_weight, mixer_gain, up_weight, down_weight
):
    rows, wide = queries.shape[0], queries.shape[1] // 2
    depth, units = up_weight.shape
    cols = down_weight.shape[1]
    piece, width = tokens.shape
    total = 2 * rows
    vmem = pl.BlockSpec(memory_space=pltpu.VMEM)
    dma = pltpu.SemaphoreType.DMA
    return pl.pallas_call(
        functools.partial(layer_kernel, n, tp),
        out_shape=jax.ShapeDtypeStruct(tokens.shape, bf16),
        in_specs=[pl.BlockSpec(memory_space=pltpu.SMEM)] + [vmem] * 8 + [pl.BlockSpec(memory_space=pl.ANY)],
        out_specs=vmem,
        scratch_shapes=[
            pltpu.VMEM((tp, piece, 2 * tp * wide), bf16),
            pltpu.VMEM((n * depth, units), bf16),
            pltpu.VMEM((n, units, cols), bf16),
            pltpu.VMEM((2, total, wide), bf16),
            pltpu.VMEM((n // 2, 2, total, wide), bf16),
            pltpu.VMEM((2, 2 * total, wide), bf16),
            pltpu.VMEM((2, 2 * total, 128), f32),
            pltpu.VMEM((2, 2 * total, 128), f32),
            pltpu.VMEM((2, 2 * total, wide), f32),
            pltpu.VMEM((tp, 2, piece, wide), bf16),
            pltpu.VMEM((tp, 2, piece, wide), bf16),
            pltpu.VMEM(out_weight.shape, bf16),
            pltpu.VMEM((rows, width), bf16),
            pltpu.VMEM((rows, width), bf16),
            pltpu.VMEM((rows, units), f32),
            pltpu.VMEM((rows, units), bf16),
            pltpu.VMEM((n, rows, cols), bf16),
            pltpu.VMEM((n, 2, piece, cols), bf16),
            pltpu.VMEM((n, piece, cols), bf16),
            pltpu.VMEM((n, piece, cols), bf16),
            dma((2, 3)), dma((3,)), dma((2, 3)), dma((CHUNKS,)), dma((3,)), dma((tp,)),
            dma((n // 2,)), dma((n // 2,)),
            dma((n, CHUNKS)), dma((CHUNKS,)), dma((n, CHUNKS)), dma((n, CHUNKS)), dma((1,)), dma((1,)),
            dma((2 * tp,)), dma((2 * tp,)), dma((8,)),
            dma((n, 2)), dma((n, 2)), dma((n,)), dma((n,)),
        ],
        compiler_params=pltpu.CompilerParams(
            collective_id=0, has_side_effects=True, vmem_limit_bytes=60 * 1024 * 1024
        ),
    )(
        lambdas, queries, keys, values, head_gain.reshape(1, -1), up_weight, down_weight,
        tokens, mixer_gain.reshape(1, -1), out_weight,
    )


def solution(mesh):
    placed = (
        P(("sp", "tp"), None),
        P("sp", "tp"),
        P("sp", "tp"),
        P("sp", "tp"),
        P("tp"),
        P(),
        P(),
        P(),
        P("sp", "tp"),
        P("tp", "sp"),
    )
    return jax.shard_map(
        functools.partial(per_device, mesh.shape["sp"], mesh.shape["tp"]),
        mesh=mesh,
        in_specs=placed,
        out_specs=P(("sp", "tp"), None),
        check_vma=False,
    )
```

time: 136 us -> 116 us (0.85)
  Pallas kernels: 132 us -> 113 us
    pallas_call x1, Pallas kernels: 132 us -> 113 us  [per_device(): pl.pallas_call(functools.partial(layer_kernel, n, tp), out_shape=jax.Shap...]
where the time goes in v1:
time: 116 us; the launch traced here: 115 us
  Pallas kernels  113 us (97%)
  local copies, waits for them, and re-layouts  1.88 us (2%)
    pallas_call x1, Pallas kernels, per_device(): pl.pallas_call(functools.partial(layer_kernel, n, tp), out_shape=jax.Shap...  113 us

profile of v1, /device:TPU:25, one launch (start us, length us, event | category | flops | bytes accessed | tf_op | source)
XLA Modules:
  0.0 114.8 jit_solution(736149940907955687)
XLA Ops:
  0.0 112.9 %shard_map.100 = bf16[128,2048]{1,0:T(8,128)(2,1)} custom-call(f32[2]{0:T(128)} %lam_ref.1, bf16[512,256]{1,0:T(8,128)(2,1)} %q_ref.1, bf16[512,256]{1,0:T(8,128)(2,1)} %k_ref.1, bf16[512,256]{1,0:T(8,128)(2,1)} %v_ref.1, f32[1,128]{1,0:T(1,128)} %bitcast.3, bf16[256,1024]{1,0:T(8,128)(2,1)} %up_ref.1, bf16[1024,256]{1,0:T(8,128)(2,1)} %dn_ref.1, ...), custom_call_target="tpu_custom_call" | custom-call | tf_op jit(solution)/shard_map/pallas_call | solution.py:579
  112.9 1.9 %copy.12 = bf16[128,2048]{1,0:T(8,128)(2,1)} copy(bf16[128,2048]{1,0:T(8,128)(2,1)} %shard_map.100) | data formatting | bytes 1048576

commit v2 on v1

--- a/solution.py
+++ b/solution.py
@@ -39,7 +39,6 @@
     beside = (s + 1 - 2 * y, t)
     core = (s, t + 1 - 2 * c)
     across_x = (s, lax.rem(t + 2, tp))
-    corner = (s + 1 - 2 * y, lax.rem(t + 2, tp))
     line = 2 * z + c
     own_line = y == c
     partner = (line, 2 * x + y)
@@ -59,13 +58,7 @@
 
     pl.when(has_up)(lambda: greet(above))
     pl.when(has_down)(lambda: greet(below))
-    pl.when(top)(lambda: greet((s - 2 + 1 - 2 * y, t)))
-    pl.when(helper)(lambda: greet((s + 2 + 1 - 2 * y, t)))
-    pl.semaphore_wait(
-        barrier,
-        2 * tp - 1 + has_up.astype(jnp.int32) + has_down.astype(jnp.int32)
-        + jnp.logical_or(top, helper).astype(jnp.int32),
-    )
+    pl.semaphore_wait(barrier, 2 * tp - 1 + has_up.astype(jnp.int32) + has_down.astype(jnp.int32))
 
     def remote(src, dst, send, recv, device):
         return pltpu.make_async_remote_copy(
@@ -91,22 +84,32 @@
         )
 
     def lower(i, e):
-        cols = my_cols if e == 0 else peer_cols
-        device = below if e == 0 else (s - 2 + 1 - 2 * y, t)
+        where = my_rows if e == 0 else peer_rows
+        src = qkv[i].at[:, my_cols] if e == 0 else landing(i, z, 0, where)
+        return remote(src, landing(i, z, 1, where), ex_send.at[1 + e, i], top_recv.at[y if e == 0 else 1 - y, i], below)
+
+    def kv_part(j, r, i):
+        part_of = kv.at[j, i, rows_of(r)]
+        return remote(part_of, part_of, kv_send.at[j, r, i], kv_recv.at[j, r, i], above)
+
+    def own_kv(i):
         return remote(
-            qkv[i].at[:, cols], landing(i, z, 1, my_rows), ex_send.at[e, i], top_recv.at[y, i], device
+            qkv[1 + i].at[:, my_cols], kv.at[z, i, my_rows], kv_send.at[z, y, i], kv_recv.at[z, y, i], above
         )
 
-    @pl.when(jnp.logical_not(top))
-    def _():
-        for i in (1, 2, 0):
-            exchange(i, my_rows).start()
+    kv_rises = z < steps - 2
+    for i in (1, 2, 0):
+        exchange(i, my_rows).start()
+
+    @pl.when(kv_rises)
+    def _():
+        for i in range(2):
+            own_kv(i).start()
 
     @pl.when(top)
     def _():
         for i in range(3):
-            for e in range(2):
-                lower(i, e).start()
+            lower(i, 0).start()
 
     depth, units = up_ref.shape
     half_depth, half = depth // 2, units // 2
@@ -146,8 +149,7 @@
     def _():
         for k in UPS:
             own_above(k, given[k])
-        for k in UPS + DOWNS:
-            own_around(k, given[k])
+            pl.when(jnp.logical_not(top))(lambda: own_around(k, given[k]))
 
     @pl.when(jnp.logical_not(own_line))
     def _():
@@ -162,10 +164,17 @@
     by = lax.rem(b + 2, tp)
     bd = lax.rem(bx + 2, tp)
 
-    def token_copy(k, source, device):
-        return remote(tok_ref, tokall.at[band(source)], tk_send.at[k], tk_recv.at[source], device)
-
-    token_copy(0, b, across_x).start()
+    half_piece = piece // 2
+
+    def token_own(k):
+        return remote(tok_ref, tokall.at[band(b)], tk_send.at[k], tk_recv.at[k], (across_x, beside)[k])
+
+    def token_half(k):
+        source = (bx, by)[k]
+        moved = tokall.at[pl.ds(pl.multiple_of(source * piece + k * half_piece, half_piece), half_piece)]
+        return remote(moved, moved, tk_send.at[2 + k], tk_recv.at[2 + k], (beside, across_x)[k])
+
+    token_own(0).start()
 
     def local_copy(i):
         src, dst = (
@@ -179,10 +188,8 @@
         )[i]
         return pltpu.make_async_copy(src, dst, loc.at[i])
 
-    @pl.when(jnp.logical_not(top))
-    def _():
-        for i in range(3):
-            local_copy(i).start()
+    for i in range(3):
+        local_copy(i).start()
 
     @pl.when(own_line)
     def _():
@@ -192,27 +199,32 @@
     local_copy(5).start()
     local_copy(6).start()
 
-    def kv_up(j):
-        return remote(kv.at[j], kv.at[j], kv_send.at[j], kv_recv.at[j], above)
-
-    kv_rises = z < steps - 2
-
-    @pl.when(jnp.logical_not(top))
+    for i in range(3):
+        local_copy(i).wait()
+    for i in (1, 2, 0):
+        exchange(i, peer_rows).wait_recv()
+        if i > 0:
+            pl.when(kv_rises)(lambda: kv_part(z, 1 - y, i - 1).start())
+
+    @pl.when(top)
     def _():
         for i in range(3):
-            local_copy(i).wait()
-        for i in (1, 2, 0):
-            exchange(i, peer_rows).wait_recv()
-        pl.when(kv_rises)(lambda: kv_up(z).start())
-
-    @pl.when(jnp.logical_and(own_line, early_down))
-    def _():
+            lower(i, 1).start()
+
+    @pl.when(own_line)
+    def _():
+        for k in UPS:
+            pl.when(top)(lambda: own_around(k, given[k]))
         for k in DOWNS:
-            own_above(k, given[k])
+            pl.when(early_down)(lambda: own_above(k, given[k]))
+            own_around(k, given[k])
 
     def await_chunk(k, j):
         moved = shard(k, j)
         remote(moved, moved, w_send.at[j, k], w_recv.at[j, k], core).wait_recv()
+
+    def from_core(k, i):
+        await_chunk(k, 2 * i + 1 - c)
 
     def swapped(ks):
         @pl.when(jnp.logical_not(own_line))
@@ -334,24 +346,41 @@
     @pl.when(helper)
     def _():
         lax.fori_loop(1, 2, diagonal, 0)
+        swapped(DOWNS)
         tiles(1, z)
 
-    swapped(DOWNS)
-    token_copy(1, b, beside).start()
-    token_copy(2, b, corner).start()
+    def spread():
+        pl.when(jnp.logical_not(helper))(lambda: swapped(DOWNS))
+
+        @pl.when(own_line)
+        def _():
+            for k in DOWNS:
+                from_core(k, z)
+
+        token_own(1).start()
+        token_own(0).wait_recv()
+        token_half(0).start()
+
+    middle = jnp.logical_and(z > 0, kv_rises)
+    def pass_tokens():
+        token_own(1).wait_recv()
+        token_half(1).start()
+
+    pl.when(jnp.logical_not(middle))(spread)
 
     def block(d, carry):
         j = z - d
-        kv_up(j).wait_recv()
-        pl.when(kv_rises)(lambda: kv_up(j).start())
+        for r in (y, 1 - y):
+            for i in range(2):
+                kv_part(j, r, i).wait_recv()
+                pl.when(kv_rises)(lambda: kv_part(j, r, i).start())
+
+        pl.when(d == jnp.where(helper, 1, 2))(lambda: from_below(1, UPS))
 
         def slot(v, inner):
             u = 1 - v
-
-            @pl.when(jnp.logical_and(u == 0, d == 2))
-            def _():
-                from_below(1, UPS)
-
+            own_turn = jnp.logical_and(u == 0, d == 1)
+            pl.when(jnp.logical_and(own_turn, helper))(lambda: from_above(1, UPS))
             tiles(u, j)
 
             @pl.when(jnp.logical_and(u == 1, d == z))
@@ -362,7 +391,8 @@
             return inner
 
         lax.fori_loop(jnp.where(helper, 0, 1), 2, slot, 0)
-        pl.when(d == 1)(lambda: from_above(1, UPS))
+        pl.when(jnp.logical_and(d == 1, middle))(spread)
+        pl.when(jnp.logical_and(d == 1, kv_rises))(lambda: from_above(1, UPS))
         pl.when(d == 2)(lambda: from_above(1, DOWNS))
         return carry
 
@@ -371,7 +401,9 @@
 
     @pl.when(top)
     def _():
-        from_below(1, UPS + DOWNS)
+        from_below(1, UPS)
+        pass_tokens()
+        from_below(1, DOWNS)
         from_below(2, UPS)
         raise_att().wait_recv()
 
@@ -394,16 +426,22 @@
     @pl.when(z == 0)
     def _():
         from_above(1, UPS + DOWNS)
+        pass_tokens()
 
     @pl.when(z == 1)
     def _():
-        from_above(1, DOWNS)
         from_below(1, UPS)
         late_down()
+        from_above(1, DOWNS[:1])
+        pass_tokens()
+        from_above(2, UPS)
+        from_above(1, DOWNS[1:])
 
     @pl.when(jnp.logical_and(z >= 2, has_up))
     def _():
+        pass_tokens()
         from_below(2, UPS)
+        pl.when(helper)(lambda: from_below(1, DOWNS))
 
     @pl.when(top)
     def _():
@@ -412,8 +450,9 @@
     local_copy(5).wait()
     local_copy(6).wait()
     mine.wait()
-    for k, (source, device) in enumerate(((bx, across_x), (by, beside), (bd, corner))):
-        token_copy(k, source, device).wait_recv()
+    for k in range(2):
+        token_half(k).wait_recv()
+        token_half(k).wait_send()
     for i in range(2 * tp):
         e, who = i % 2, i // 2
         pl.when(jnp.logical_or(e != y, who != t))(lambda: to_tokens(0, 0, i).wait_recv())
@@ -432,14 +471,14 @@
     lax.fori_loop(0, tp // 2, project, 0)
 
     def later_ups(d, carry):
-        pl.when(z + d < steps)(lambda: from_above(d, UPS))
+        pl.when(jnp.logical_and(z + d < steps, jnp.logical_or(z != 1, d != 2)))(lambda: from_above(d, UPS))
         waits = jnp.logical_and(d >= 3, jnp.logical_not(jnp.logical_and(top, d == 3)))
         pl.when(jnp.logical_and(z - d >= 0, waits))(lambda: from_below(d, UPS))
         return carry
 
     lax.fori_loop(2, steps, later_ups, 0)
     pl.when(jnp.logical_and(z > 1, kv_rises))(late_down)
-    pl.when(jnp.logical_and(z >= 1, has_up))(lambda: from_below(1, DOWNS))
+    pl.when(jnp.logical_and(z >= 1, kv_rises))(lambda: from_below(1, DOWNS))
 
     @pl.when(own_line)
     def _():
@@ -448,9 +487,6 @@
 
     def order(k):
         return jnp.where(k < steps - z, z + k, steps - 1 - k)
-
-    def from_core(k, i):
-        await_chunk(k, 2 * i + 1 - c)
 
     pair_depth = 2 * depth
     hsum[...] = jnp.zeros_like(hsum)
@@ -487,21 +523,29 @@
 
     def down_pair(k, carry):
         i = order(k)
-        last = k == steps - 1
-        pl.when(last)(lambda: relay(order(k - 1)))
+        early = jnp.logical_and(k == steps - 1, jnp.logical_or(top, z == 0))
+
+        @pl.when(early)
+        def _():
+            relay(order(k - 2))
+            relay(order(k - 1))
+
         pl.when(i - z >= 2)(lambda: from_above(i - z, DOWNS))
-        pl.when(z - i >= 2)(lambda: from_below(z - i, DOWNS))
+        pl.when(z - i >= jnp.where(helper, 3, 2))(lambda: from_below(z - i, DOWNS))
         for m in DOWNS:
-            from_core(m, i)
+            pl.when(jnp.logical_and(helper, k == m - 1))(lambda: from_below(2, (m,)))
+        for m in DOWNS:
+            pl.when(jnp.logical_not(jnp.logical_and(own_line, i == z)))(lambda: from_core(m, i))
         for e in range(2):
             j = 2 * i + e
             part[j] = jnp.dot(hid[...], dnf_ref[j], preferred_element_type=f32).astype(bf16)
             to_first(j, e, 1).start()
             to_first(j, e, 0).start()
-        pl.when(jnp.logical_and(k > 0, k < steps - 1))(lambda: relay(order(k - 1)))
+        pl.when(jnp.logical_and(k > 1, jnp.logical_not(early)))(lambda: relay(order(k - 2)))
         return carry
 
     lax.fori_loop(0, steps, down_pair, 0)
+    pl.when(jnp.logical_not(jnp.logical_or(top, z == 0)))(lambda: relay(order(steps - 2)))
     relay(order(steps - 1))
 
     cols = dn_ref.shape[1]
@@ -516,16 +560,14 @@
         to_first(j, j % 2, 0).wait_send()
         to_first(j, j % 2, 1).wait_send()
         to_second(j, j % 2).wait_send()
-    for k, device in enumerate((across_x, beside, corner)):
-        token_copy(k, b, device).wait_send()
+    for k in range(2):
+        token_own(k).wait_send()
     for e in range(2):
         for i in range(tp):
             pl.when(jnp.logical_or(e != y, i != t))(lambda: to_tokens(e, i, head).wait_send())
 
-    @pl.when(jnp.logical_not(top))
-    def _():
-        for i in range(3):
-            exchange(i, my_rows).wait_send()
+    for i in range(3):
+        exchange(i, my_rows).wait_send()
 
     @pl.when(top)
     def _():
@@ -543,7 +585,9 @@
     @pl.when(kv_rises)
     def _():
         def sent(j, carry):
-            kv_up(j).wait_send()
+            for r in range(2):
+                for i in range(2):
+                    kv_part(j, r, i).wait_send()
             return carry
 
         lax.fori_loop(0, z + 1, sent, 0)
@@ -602,8 +646,8 @@
             pltpu.VMEM((n, 2, piece, cols), bf16),
             pltpu.VMEM((n, piece, cols), bf16),
             pltpu.VMEM((n, piece, cols), bf16),
-            dma((2, 3)), dma((3,)), dma((2, 3)), dma((CHUNKS,)), dma((3,)), dma((tp,)),
-            dma((n // 2,)), dma((n // 2,)),
+            dma((3, 3)), dma((3,)), dma((2, 3)), dma((CHUNKS,)), dma((4,)), dma((4,)),
+            dma((n // 2, 2, 2)), dma((n // 2, 2, 2)),
             dma((n, CHUNKS)), dma((CHUNKS,)), dma((n, CHUNKS)), dma((n, CHUNKS)), dma((1,)), dma((1,)),
             dma((2 * tp,)), dma((2 * tp,)), dma((8,)),
             dma((n, 2)), dma((n, 2)), dma((n,)), dma((n,)),

time: 116 us -> 103 us (0.89)
  Pallas kernels: 113 us -> 101 us
    pallas_call x1, Pallas kernels: 113 us -> 101 us  [per_device(): pl.pallas_call(functools.partial(layer_kernel, n, tp), out_shape=jax.Shap...]
where the time goes in v2:
time: 103 us; the launch traced here: 102 us
  Pallas kernels  101 us (98%)
  local copies, waits for them, and re-layouts  1.88 us (2%)
    pallas_call x1, Pallas kernels, per_device(): pl.pallas_call(functools.partial(layer_kernel, n, tp), out_shape=jax.Shap...  101 us

profile of v2, /device:TPU:25, one launch (start us, length us, event | category | flops | bytes accessed | tf_op | source)
XLA Modules:
  0.0 102.4 jit_solution(17153202865084525340)
XLA Ops:
  0.0 100.5 %shard_map.100 = bf16[128,2048]{1,0:T(8,128)(2,1)} custom-call(f32[2]{0:T(128)} %lam_ref.1, bf16[512,256]{1,0:T(8,128)(2,1)} %q_ref.1, bf16[512,256]{1,0:T(8,128)(2,1)} %k_ref.1, bf16[512,256]{1,0:T(8,128)(2,1)} %v_ref.1, f32[1,128]{1,0:T(1,128)} %bitcast.3, bf16[256,1024]{1,0:T(8,128)(2,1)} %up_ref.1, bf16[1024,256]{1,0:T(8,128)(2,1)} %dn_ref.1, ...), custom_call_target="tpu_custom_call" | custom-call | tf_op jit(solution)/shard_map/pallas_call | solution.py:623
  100.5 1.9 %copy.12 = bf16[128,2048]{1,0:T(8,128)(2,1)} copy(bf16[128,2048]{1,0:T(8,128)(2,1)} %shard_map.100) | data formatting | bytes 1048576

commit v3 on v2

v3 whole, which is shorter than its diff:
```python
import functools

import jax
import jax.numpy as jnp
from jax import lax
from jax.experimental import pallas as pl
from jax.experimental.pallas import tpu as pltpu
from jax.sharding import PartitionSpec as P

DQK = 64
MESH = pl.DeviceIdType.MESH
f32, bf16 = jnp.float32, jnp.bfloat16
CHUNKS = 4
UPS, DOWNS = (0, 1), (2, 3)


def layer_kernel(
    n, tp,
    lam_ref, gain_ref, mix_ref, q_hbm, k_hbm, v_hbm, up_hbm, dn_hbm, tok_hbm, ow_hbm,
    out_hbm,
    q_ref, k_ref, v_ref, up_ref, dn_ref, tok_ref,
    ah, upf_ref, dnf_ref,
    qb, kv, qm, run_max, run_sum, acc, att, ow, tokall, normed, hid, part, core_in, cross, cross_in, out_rows,
    ex_send, ex_recv, top_recv, swap_send, tk_send, tk_recv, kv_send, kv_recv,
    w_send, own_send, y_send, w_recv, u_send, u_recv, a_send, a_recv, loc, own_att, put_sem, in_sem,
    c_send, first_recv, c_recv, x_send, x_recv,
):
    s = lax.axis_index("sp")
    t = lax.axis_index("tp")
    z, y = s // 2, lax.rem(s, 2)
    x, c = t // 2, lax.rem(t, 2)
    steps = n // 2
    rows = q_ref.shape[0]
    wide = q_ref.shape[1] // 2
    total = 2 * rows
    piece = rows // tp
    top, helper = z == steps - 1, z == steps - 2
    has_up, has_down = z < steps - 1, z > 0
    above, below = (s + 2, t), (s - 2, t)
    beside = (s + 1 - 2 * y, t)
    core = (s, t + 1 - 2 * c)
    across_x = (s, lax.rem(t + 2, tp))
    line = 2 * z + c
    own_line = y == c
    partner = (line, 2 * x + y)

    fetched = []
    for i, (src, dst) in enumerate((
        (k_hbm, k_ref), (v_hbm, v_ref), (q_hbm, q_ref), (up_hbm, up_ref), (dn_hbm, dn_ref), (tok_hbm, tok_ref)
    )):
        fetched.append(pltpu.make_async_copy(src, dst, in_sem.at[i]))
        fetched[-1].start()

    barrier = pltpu.get_barrier_semaphore()

    def greet(device):
        pl.semaphore_signal(barrier, inc=1, device_id=device, device_id_type=MESH)

    for e in range(2):
        for i in range(tp):
            who = (2 * z + e, i)

            @pl.when(jnp.logical_or(e != y, i != t))
            def _():
                greet(who)

    pl.when(has_up)(lambda: greet(above))
    pl.when(has_down)(lambda: greet(below))
    pl.semaphore_wait(barrier, 2 * tp - 1 + has_up.astype(jnp.int32) + has_down.astype(jnp.int32))

    for copy in fetched:
        copy.wait()

    def remote(src, dst, send, recv, device):
        return pltpu.make_async_remote_copy(
            src_ref=src, dst_ref=dst, send_sem=send, recv_sem=recv, device_id=device, device_id_type=MESH
        )

    def drain(ref, sem):
        remote(ref, ref, sem, sem, beside).wait_send()

    def rows_of(e):
        return pl.ds(pl.multiple_of(e * rows, rows), rows)

    def cols_of(e):
        return pl.ds(pl.multiple_of(e * wide, wide), wide)

    my_rows, peer_rows = rows_of(y), rows_of(1 - y)
    my_cols, peer_cols = cols_of(y), cols_of(1 - y)
    qkv = (q_ref, k_ref, v_ref)

    def landing(i, plane, slot, where):
        return qb.at[slot, where] if i == 0 else kv.at[plane, i - 1, where]

    def exchange(i, where):
        return remote(
            qkv[i].at[:, peer_cols], landing(i, z, 0, where), ex_send.at[0], ex_recv.at[i], beside
        )

    def lower(i, e):
        where = my_rows if e == 0 else peer_rows
        src = qkv[i].at[:, my_cols] if e == 0 else landing(i, z, 0, where)
        return remote(src, landing(i, z, 1, where), ex_send.at[1 + e], top_recv.at[y if e == 0 else 1 - y], below)

    def kv_part(j, r, i):
        part_of = kv.at[j, i, rows_of(r)]
        return remote(part_of, part_of, kv_send.at[j], kv_recv.at[j, r], above)

    def own_kv(i):
        return remote(
            qkv[1 + i].at[:, my_cols], kv.at[z, i, my_rows], kv_send.at[z], kv_recv.at[z, y], above
        )

    kv_rises = z < steps - 2
    for i in (1, 2, 0):
        exchange(i, my_rows).start()

    @pl.when(kv_rises)
    def _():
        for i in range(2):
            own_kv(i).start()

    @pl.when(top)
    def _():
        for i in range(3):
            lower(i, 0).start()

    depth, units = up_ref.shape
    half_depth, half = depth // 2, units // 2

    def shard(k, j):
        if k in UPS:
            return upf_ref.at[pl.ds(pl.multiple_of(j * depth + k * half_depth, half_depth), half_depth)]
        return dnf_ref.at[j, slice((k - 2) * half, (k - 1) * half)]

    given = (
        up_ref.at[slice(0, half_depth)], up_ref.at[slice(half_depth, depth)],
        dn_ref.at[slice(0, half)], dn_ref.at[slice(half, units)],
    )

    def swap(k):
        return remote(given[k], shard(k, s), swap_send.at[0], w_recv.at[s, k], partner)

    def send_above(k, j, src):
        remote(src, shard(k, j), w_send.at[j], w_recv.at[j, k], above).start()

    def send_below(k, j, src, sems):
        remote(src, shard(k, j), sems, w_recv.at[j, k], below).start()

    def over(k, j, src):
        remote(src, shard(k, j), y_send.at[0], w_recv.at[j, k], core).start()

    early_down = jnp.logical_or(z == 0, helper)

    def own_above(k, src):
        pl.when(has_up)(lambda: send_above(k, line, src))

    def own_around(k, src):
        pl.when(has_down)(lambda: send_below(k, line, src, own_send.at[0]))
        over(k, line, src)

    @pl.when(own_line)
    def _():
        for k in UPS:
            own_above(k, given[k])
            pl.when(jnp.logical_not(top))(lambda: own_around(k, given[k]))
        for k in DOWNS:
            pl.when(helper)(lambda: own_above(k, given[k]))

    @pl.when(jnp.logical_not(own_line))
    def _():
        for k in UPS + DOWNS:
            swap(k).start()

    b = 2 * y + x
    bx = b + 1 - 2 * x
    by = lax.rem(b + 2, tp)
    bd = lax.rem(bx + 2, tp)

    half_piece = piece // 2

    def token_own(k):
        return remote(tok_ref, tokall.at[b], tk_send.at[k], tk_recv.at[k], (across_x, beside)[k])

    def token_half(k):
        source = (bx, by)[k]
        moved = tokall.at[source, pl.ds(k * half_piece, half_piece)]
        return remote(moved, moved, tk_send.at[2 + k], tk_recv.at[2 + k], (beside, across_x)[k])

    token_own(0).start()

    def local_copy(i):
        src, dst = (
            (k_ref.at[:, my_cols], kv.at[z, 0, my_rows]),
            (v_ref.at[:, my_cols], kv.at[z, 1, my_rows]),
            (q_ref.at[:, my_cols], qb.at[0, my_rows]),
            (up_ref, upf_ref.at[pl.ds(pl.multiple_of(s * depth, depth), depth)]),
            (dn_ref, dnf_ref.at[s]),
            (ow_hbm, ow),
            (tok_ref, tokall.at[b]),
        )[i]
        return pltpu.make_async_copy(src, dst, loc.at[i])

    for i in range(3):
        local_copy(i).start()

    @pl.when(own_line)
    def _():
        local_copy(3).start()
        local_copy(4).start()

    local_copy(5).start()
    local_copy(6).start()

    for i in range(3):
        local_copy(i).wait()
    for i in (1, 2, 0):
        exchange(i, peer_rows).wait_recv()
        if i > 0:
            pl.when(kv_rises)(lambda: kv_part(z, 1 - y, i - 1).start())

    @pl.when(top)
    def _():
        for i in range(3):
            lower(i, 1).start()

    @pl.when(own_line)
    def _():
        for k in UPS:
            pl.when(top)(lambda: own_around(k, given[k]))
        for k in DOWNS:
            pl.when(z == 0)(lambda: own_above(k, given[k]))
            own_around(k, given[k])

    def await_chunk(k, j):
        moved = shard(k, j)
        remote(moved, moved, w_send.at[j], w_recv.at[j, k], core).wait_recv()

    def from_core(k, i):
        await_chunk(k, 2 * i + 1 - c)

    def swapped(ks):
        @pl.when(jnp.logical_not(own_line))
        def _():
            for k in ks:
                await_chunk(k, line)
                src = shard(k, line)
                if k in UPS:
                    own_above(k, src)
                else:
                    pl.when(early_down)(lambda: own_above(k, src))
                own_around(k, src)

    def late_down():
        @pl.when(own_line)
        def _():
            for k in DOWNS:
                own_above(k, given[k])

        @pl.when(jnp.logical_not(own_line))
        def _():
            for k in DOWNS:
                own_above(k, shard(k, line))

    def from_above(d, ks):
        j = line + 2 * d
        for k in ks:
            await_chunk(k, j)
            src = shard(k, j)
            pl.when(has_down)(lambda: send_below(k, j, src, w_send.at[j]))
            over(k, j, src)

    def from_below(d, ks):
        j = line - 2 * d
        for k in ks:
            await_chunk(k, j)
            src = shard(k, j)
            pl.when(has_up)(lambda: send_above(k, j, src))
            over(k, j, src)

    chunk = rows
    lane = lax.broadcasted_iota(jnp.int32, (total, wide), 1)

    def weigh(sc, top_row):
        parts, whole = [], None
        for i in range(sc.shape[1] // 128):
            p = jnp.exp(sc[:, i * 128:(i + 1) * 128] - top_row)
            whole = p if whole is None else whole + p
            parts.append(p.astype(bf16))
        return jnp.concatenate(parts, axis=1), whole

    def scores_of(u, r0, j, keys):
        return lax.dot_general(
            qm[u, pl.ds(r0, chunk), :], kv[j, 0, :keys, :], (((1,), (1,)), ((), ())), preferred_element_type=f32
        )

    def diagonal(u, carry):
        @pl.when(u == 1)
        def _():
            for e in range(2):
                three = qm.at[1, slice(0, 3 * rows)]
                remote(three, three, ex_send.at[0], top_recv.at[e], above).wait_recv()

        scaled = qb[u] * jnp.asarray(DQK ** -0.5, bf16)
        for m in range(2):
            qm[u, m * total:(m + 1) * total, :] = jnp.where((lane < DQK) == (m == 0), scaled, jnp.zeros_like(scaled))
        j = z + u
        for m in range(2):
            for i in range(total // chunk):
                r0, keys = m * total + i * chunk, (i + 1) * chunk
                here = pl.ds(r0, chunk)
                sc = scores_of(u, r0, j, keys)
                qpos = i * chunk + lax.broadcasted_iota(jnp.int32, (chunk, keys), 0)
                kpos = lax.broadcasted_iota(jnp.int32, (chunk, keys), 1)
                sc = jnp.where(kpos <= qpos, sc, -jnp.inf)
                top_row = jnp.broadcast_to(jnp.max(sc, axis=1, keepdims=True), (chunk, 128))
                p, whole = weigh(sc, top_row)
                run_max[u, here, :] = top_row
                run_sum[u, here, :] = whole
                acc[u, here, :] = jnp.dot(p, kv[j, 1, :keys, :], preferred_element_type=f32)
        return carry

    def tile(u, j, r0):
        here = pl.ds(r0, chunk)
        sc = scores_of(u, r0, j, total)
        old = run_max[u, here, :]
        top_row = jnp.maximum(old, jnp.max(sc, axis=1, keepdims=True))
        p, whole = weigh(sc, top_row)
        shrink = jnp.exp(old - top_row)
        run_max[u, here, :] = top_row
        run_sum[u, here, :] = run_sum[u, here, :] * shrink + whole
        acc[u, here, :] = acc[u, here, :] * shrink + jnp.dot(p, kv[j, 1], preferred_element_type=f32)

    def tiles(u, j, hh):
        def one(m, carry):
            tile(u, j, pl.multiple_of(m * total + hh * rows, rows))
            return carry

        lax.fori_loop(0, 2, one, 0)

    def finish(u, hh):
        lam = lam_ref[y]
        maps = []
        for m in range(2):
            here = pl.ds(pl.multiple_of(m * total + hh * rows, rows), rows)
            maps.append(acc[u, here, :] / jnp.sum(run_sum[u, here, :], axis=1, keepdims=True))
        differ = maps[0] - lam * maps[1]
        spread_of = lax.rsqrt(jnp.mean(differ * differ, axis=1, keepdims=True) + 1e-06)
        done = (differ * spread_of * gain_ref[...]).astype(bf16)
        att[u, pl.ds(hh * (tp // 2), tp // 2)] = done.reshape(tp // 2, 2, piece, wide)

    def side(hh):
        return pl.ds(hh * (tp // 2), tp // 2)

    def raise_att(hh):
        return remote(att.at[1, side(hh)], att.at[0, side(hh)], u_send.at[hh], u_recv.at[hh], above)

    head = 2 * t + y

    def head_cols(i):
        return pl.ds(pl.multiple_of(i * wide, wide), wide)

    def to_tokens(hh, e, i, owner):
        return remote(
            att.at[0, side(hh), i % 2], ah.at[side(hh), :, head_cols(owner)],
            a_send.at[0], a_recv.at[0], (2 * z + e, i),
        )

    def mine(hh):
        return pltpu.make_async_copy(
            att.at[0, side(hh), c], ah.at[side(hh), :, head_cols(head)], own_att.at[hh]
        )

    def hand_out(hh):
        mine(hh).start()
        for e in range(2):
            for i in range(tp):
                pl.when(jnp.logical_or(e != y, i != t))(lambda: to_tokens(hh, e, i, head).start())

    def spread():
        swapped(DOWNS)

        @pl.when(own_line)
        def _():
            for k in DOWNS:
                from_core(k, z)

        token_own(1).start()
        token_own(0).wait_recv()
        token_half(0).start()

    def pass_tokens():
        token_own(1).wait_recv()
        token_half(1).start()

    @pl.when(jnp.logical_not(top))
    def _():
        diagonal(0, 0)

    swapped(UPS)
    forwarded = jnp.logical_and(helper, own_line)
    pl.when(forwarded)(lambda: from_below(1, UPS))

    @pl.when(helper)
    def _():
        lax.fori_loop(1, 2, diagonal, 0)
        spread()
        for hh in range(2):
            tiles(1, z, hh)

    middle = jnp.logical_and(z > 0, kv_rises)
    pl.when(jnp.logical_or(z == 0, top))(spread)

    def block(d, carry):
        j = z - d
        for r in (y, 1 - y):
            moved = kv.at[j, :, rows_of(r)]
            remote(moved, moved, kv_send.at[j], kv_recv.at[j, r], above).wait_recv()
            for i in range(2):
                pl.when(kv_rises)(lambda: kv_part(j, r, i).start())

        forward_now = jnp.logical_and(d == jnp.where(helper, 1, 2), jnp.logical_not(forwarded))
        pl.when(forward_now)(lambda: from_below(1, UPS))

        def slot(v, inner):
            u, hh = 1 - v // 2, lax.rem(v, 2)
            own_turn = jnp.logical_and(v == 2, helper)
            pl.when(jnp.logical_and(own_turn, d == 1))(lambda: from_above(1, UPS))
            pl.when(jnp.logical_and(own_turn, d == 2))(pass_tokens)
            tiles(u, j, hh)

            @pl.when(d == z)
            def _():
                finish(u, hh)
                pl.when(u == 1)(lambda: raise_att(hh).start())
                pl.when(u == 0)(lambda: hand_out(hh))

            return inner

        lax.fori_loop(jnp.where(helper, 0, 2), 4, slot, 0)
        pl.when(jnp.logical_and(d == 1, middle))(spread)
        pl.when(jnp.logical_and(d == 1, kv_rises))(lambda: from_above(1, UPS))
        pl.when(d == 2)(lambda: from_above(1, DOWNS))
        return carry

    lax.fori_loop(1, jnp.where(top, 1, z + 1), block, 0)

    @pl.when(z == 0)
    def _():
        for hh in range(2):
            finish(0, hh)
            hand_out(hh)

    @pl.when(top)
    def _():
        from_below(1, UPS)
        pass_tokens()
        from_below(1, DOWNS)
        from_below(2, UPS)
        for hh in range(2):
            raise_att(hh).wait_recv()
            hand_out(hh)

    @pl.when(z == 0)
    def _():
        from_above(1, UPS + DOWNS)
        pass_tokens()

    @pl.when(z == 1)
    def _():
        from_below(1, UPS)
        late_down()
        from_above(1, DOWNS[:1])
        pass_tokens()
        from_above(2, UPS)
        from_above(1, DOWNS[1:])

    @pl.when(jnp.logical_and(z >= 2, has_up))
    def _():
        pl.when(jnp.logical_not(helper))(pass_tokens)
        from_below(2, UPS)
        pl.when(helper)(lambda: from_below(1, DOWNS[:1]))

    @pl.when(top)
    def _():
        from_below(3, UPS)

    local_copy(5).wait()
    local_copy(6).wait()
    for hh in range(2):
        mine(hh).wait()
    for k in range(2):
        token_half(k).wait_recv()
        token_half(k).wait_send()
    others = ah.at[:, :, slice(0, (2 * tp - 1) * wide)]
    remote(others, others, a_send.at[0], a_recv.at[0], beside).wait_recv()

    def project(hf):
        part_rows = slice(hf * half_piece, (hf + 1) * half_piece)
        heads = ah[:, part_rows, :].reshape(2 * piece, 2 * tp * wide)
        projected = jnp.dot(heads, ow[...], preferred_element_type=f32).astype(bf16)
        given_tokens = tokall[:, part_rows, :].reshape(projected.shape).astype(f32)
        summed = (given_tokens + projected.astype(f32)).astype(bf16)
        tokall[:, part_rows, :] = summed.reshape(tp, half_piece, summed.shape[1])
        summed = summed.astype(f32)
        scale = lax.rsqrt(jnp.mean(summed * summed, axis=1, keepdims=True) + 1e-06)
        normed[hf] = (summed * scale * mix_ref[...]).astype(bf16)

    project(0)
    pl.when(helper)(lambda: from_below(1, DOWNS[1:]))

    def later_ups(d, carry):
        pl.when(jnp.logical_and(z + d < steps, jnp.logical_or(z != 1, d != 2)))(lambda: from_above(d, UPS))
        waits = jnp.logical_and(d >= 3, jnp.logical_not(jnp.logical_and(top, d == 3)))
        pl.when(jnp.logical_and(z - d >= 0, waits))(lambda: from_below(d, UPS))
        return carry

    lax.fori_loop(2, steps, later_ups, 0)
    pl.when(jnp.logical_and(z > 1, kv_rises))(late_down)
    pl.when(jnp.logical_and(z >= 1, kv_rises))(lambda: from_below(1, DOWNS))

    @pl.when(own_line)
    def _():
        local_copy(3).wait()
        local_copy(4).wait()

    def order(k):
        return jnp.where(k < steps - z, z + k, steps - 1 - k)

    def up_pair(k, carry):
        for m in UPS:
            from_core(m, k)
        return carry

    lax.fori_loop(0, steps, up_pair, 0)

    def unit(hf):
        inner = jnp.dot(normed[hf], upf_ref[...], preferred_element_type=f32)
        hid[hf] = jnp.square(jnp.maximum(inner, 0.0)).astype(bf16)

    first = ((across_x, bx), (beside, by))

    def to_first(j, e, m, hf):
        device, where = first[e]
        return remote(
            part.at[j, hf, where if m == 0 else bd], core_in.at[j, m, hf],
            c_send.at[0], (first_recv.at[j] if m == 0 else c_recv.at[j, hf]), device,
        )

    def to_second(j, e, hf):
        return remote(
            cross.at[j, hf], cross_in.at[j, hf], x_send.at[0], x_recv.at[j], first[1 - e][0]
        )

    def relay(i, hf):
        for e in range(2):
            j = 2 * i + e
            to_first(j, e, 1, hf).wait_recv()
            where = first[1 - e][1]
            cross[j, hf] = (part[j, hf, where].astype(f32) + core_in[j, 1, hf].astype(f32)).astype(bf16)
            to_second(j, e, hf).start()

    def multiply(i, hf):
        for e in range(2):
            j = 2 * i + e
            product = jnp.dot(hid[hf], dnf_ref[j], preferred_element_type=f32).astype(bf16)
            part[j, hf] = product.reshape(tp, half_piece, product.shape[1])
        for e in range(2):
            j = 2 * i + e
            to_first(j, e, 1, hf).start()
            to_first(j, e, 0, hf).start()

    def arrivals(k):
        i = order(k)
        pl.when(i - z >= 2)(lambda: from_above(i - z, DOWNS))
        pl.when(z - i >= jnp.where(helper, 3, 2))(lambda: from_below(z - i, DOWNS))
        for m in DOWNS:
            pl.when(jnp.logical_not(jnp.logical_and(own_line, i == z)))(lambda: from_core(m, i))

    ready = 2
    unit(0)

    def early_pair(k, carry):
        arrivals(k)
        multiply(order(k), 0)
        return carry

    lax.fori_loop(0, ready, early_pair, 0)
    project(1)
    unit(1)
    pl.when(helper)(lambda: from_below(2, DOWNS[:1]))

    def second_pair(k, carry):
        relay(order(k), 0)
        multiply(order(k), 1)
        return carry

    lax.fori_loop(0, ready, second_pair, 0)
    pl.when(helper)(lambda: from_below(2, DOWNS[1:]))
    edge = jnp.logical_or(top, z == 0)

    def relay_both(k):
        for hf in range(2):
            relay(order(k), hf)

    def late_pair(k, carry):
        final = k == steps - 1
        pl.when(jnp.logical_and(edge, final))(lambda: relay_both(k - 1))
        arrivals(k)
        for hf in range(2):
            multiply(order(k), hf)

        @pl.when(k == ready)
        def _():
            for i in range(ready):
                relay(order(i), 1)

        pl.when(jnp.logical_and(k > ready, jnp.logical_not(jnp.logical_and(edge, final))))(lambda: relay_both(k - 1))
        return carry

    lax.fori_loop(ready, steps, late_pair, 0)
    for k in range(2):
        token_own(k).wait_send()
    drain(others, a_send.at[0])
    three = qm.at[0, slice(0, 3 * rows)]
    drain(three, ex_send.at[0])

    @pl.when(top)
    def _():
        for e in range(2):
            drain(three, ex_send.at[1 + e])

    a_shard = upf_ref.at[slice(0, 2 * depth)]
    pl.when(jnp.logical_not(own_line))(lambda: drain(a_shard, swap_send.at[0]))

    @pl.when(helper)
    def _():
        for hh in range(2):
            raise_att(hh).wait_send()

    @pl.when(kv_rises)
    def _():
        def sent(j, carry):
            drain(kv.at[j], kv_send.at[j])
            return carry

        lax.fori_loop(0, z + 1, sent, 0)

    def line_sent(i, carry):
        gone = jnp.logical_or(jnp.logical_and(i <= z, has_up), jnp.logical_and(i > z, has_down))
        pl.when(gone)(lambda: drain(a_shard, w_send.at[2 * i + c]))
        return carry

    lax.fori_loop(0, steps, line_sent, 0)
    drain(upf_ref, y_send.at[0])
    pl.when(has_down)(lambda: drain(a_shard, own_send.at[0]))

    relay_both(steps - 1)
    cols = dn_ref.shape[1]
    width = out_hbm.shape[1]

    def put(i):
        here = slice(i * (width // 2), (i + 1) * (width // 2))
        return pltpu.make_async_copy(out_rows.at[:, here], out_hbm.at[:, here], put_sem.at[i])

    def close(js):
        for at, j in enumerate(js):
            mine_in = core_in.at[j, 0]
            remote(mine_in, mine_in, c_send.at[0], first_recv.at[j], beside).wait_recv()
            remote(cross_in.at[j], cross_in.at[j], x_send.at[0], x_recv.at[j], beside).wait_recv()
            here = slice(j * cols, (j + 1) * cols)
            both = part[j, :, b].astype(f32) + core_in[j, 0].astype(f32) + cross_in[j].astype(f32)
            out_rows[:, here] = (tokall[b, :, here].astype(f32) + both.reshape(piece, cols)).astype(bf16)
            if (at + 1) % (n // 2) == 0:
                put(j // (n // 2)).start()

    pl.when(z == 0)(lambda: close(tuple(range(n))))
    pl.when(z > 0)(lambda: close(tuple(range(n - 1, -1, -1))))

    drain(core_in, c_send.at[0])
    drain(cross, x_send.at[0])
    for i in range(2):
        put(i).wait()


def per_device(
    n, tp, tokens, queries, keys, values, lambdas, head_gain, out_weight, mixer_gain, up_weight, down_weight
):
    rows, wide = queries.shape[0], queries.shape[1] // 2
    depth, units = up_weight.shape
    cols = down_weight.shape[1]
    piece, width = tokens.shape
    total = 2 * rows
    vmem = pl.BlockSpec(memory_space=pltpu.VMEM)
    dma = pltpu.SemaphoreType.DMA
    return pl.pallas_call(
        functools.partial(layer_kernel, n, tp),
        out_shape=jax.ShapeDtypeStruct(tokens.shape, bf16),
        in_specs=[pl.BlockSpec(memory_space=pltpu.SMEM)] + [vmem] * 2 + [pl.BlockSpec(memory_space=pl.ANY)] * 7,
        out_specs=pl.BlockSpec(memory_space=pl.ANY),
        scratch_shapes=[
            pltpu.VMEM(queries.shape, bf16), pltpu.VMEM(keys.shape, bf16), pltpu.VMEM(values.shape, bf16),
            pltpu.VMEM(up_weight.shape, bf16), pltpu.VMEM(down_weight.shape, bf16), pltpu.VMEM(tokens.shape, bf16),
            pltpu.VMEM((tp, piece, 2 * tp * wide), bf16),
            pltpu.VMEM((n * depth, units), bf16),
            pltpu.VMEM((n, units, cols), bf16),
            pltpu.VMEM((2, total, wide), bf16),
            pltpu.VMEM((n // 2, 2, total, wide), bf16),
            pltpu.VMEM((2, 2 * total, wide), bf16),
            pltpu.VMEM((2, 2 * total, 128), f32),
            pltpu.VMEM((2, 2 * total, 128), f32),
            pltpu.VMEM((2, 2 * total, wide), f32),
            pltpu.VMEM((2, tp, 2, piece, wide), bf16),
            pltpu.VMEM(out_weight.shape, bf16),
            pltpu.VMEM((tp, piece, width), bf16),
            pltpu.VMEM((2, 2 * piece, width), bf16),
            pltpu.VMEM((2, 2 * piece, units), bf16),
            pltpu.VMEM((n, 2, tp, piece // 2, cols), bf16),
            pltpu.VMEM((n, 2, 2, piece // 2, cols), bf16),
            pltpu.VMEM((n, 2, piece // 2, cols), bf16),
            pltpu.VMEM((n, 2, piece // 2, cols), bf16),
            pltpu.VMEM((piece, width), bf16),
            dma((3,)), dma((3,)), dma((2,)), dma((1,)), dma((4,)), dma((4,)),
            dma((n // 2,)), dma((n // 2, 2)),
            dma((n,)), dma((1,)), dma((1,)), dma((n, CHUNKS)), dma((2,)), dma((2,)),
            dma((1,)), dma((1,)), dma((7,)), dma((2,)), dma((2,)), dma((6,)),
            dma((1,)), dma((n,)), dma((n, 2)), dma((1,)), dma((n,)),
        ],
        compiler_params=pltpu.CompilerParams(
            collective_id=0, has_side_effects=True, vmem_limit_bytes=60 * 1024 * 1024
        ),
    )(
        lambdas, head_gain.reshape(1, -1), mixer_gain.reshape(1, -1), queries, keys, values, up_weight, down_weight,
        tokens, out_weight,
    )


def solution(mesh):
    placed = (
        P(("sp", "tp"), None),
        P("sp", "tp"),
        P("sp", "tp"),
        P("sp", "tp"),
        P("tp"),
        P(),
        P(),
        P(),
        P("sp", "tp"),
        P("tp", "sp"),
    )
    return jax.shard_map(
        functools.partial(per_device, mesh.shape["sp"], mesh.shape["tp"]),
        mesh=mesh,
        in_specs=placed,
        out_specs=P(("sp", "tp"), None),
        check_vma=False,
    )
```

time: 103 us -> 97.8 us (0.950)
  Pallas kernels: 101 us -> 95.6 us
    pallas_call x1, Pallas kernels: 101 us -> 95.6 us  [per_device(): pl.pallas_call(functools.partial(layer_kernel, n, tp), out_shape=jax.Shap...]
where the time goes in v3:
time: 97.8 us; the launch traced here: 97.5 us
  Pallas kernels  95.6 us (98%)
  local copies, waits for them, and re-layouts  1.88 us (2%)
    pallas_call x1, Pallas kernels, per_device(): pl.pallas_call(functools.partial(layer_kernel, n, tp), out_shape=jax.Shap...  95.6 us

profile of v3, /device:TPU:25, one launch (start us, length us, event | category | flops | bytes accessed | tf_op | source)
XLA Modules:
  0.0 97.5 jit_solution(353879969293051993)
XLA Ops:
  0.0 95.6 %shard_map.100 = bf16[128,2048]{1,0:T(8,128)(2,1)} custom-call(f32[2]{0:T(128)} %lam_ref.1, f32[1,128]{1,0:T(1,128)} %bitcast.3, f32[1,2048]{1,0:T(1,128)} %bitcast.2, bf16[512,256]{1,0:T(8,128)(2,1)} %q_hbm.1, bf16[512,256]{1,0:T(8,128)(2,1)} %k_hbm.1, bf16[512,256]{1,0:T(8,128)(2,1)} %v_hbm.1, bf16[256,1024]{1,0:T(8,128)(2,1)} %up_hbm.1, ...), custom_call_target="tpu_custom_call" | custom-call | tf_op jit(solution)/shard_map/pallas_call | solution.py:696
  95.6 1.9 %copy.12 = bf16[128,2048]{1,0:T(8,128)(2,1)} copy(bf16[128,2048]{1,0:T(8,128)(2,1)} %shard_map.100) | data formatting | bytes 1048576

commit v4 on v3

--- a/solution.py
+++ b/solution.py
@@ -17,10 +17,10 @@
 def layer_kernel(
     n, tp,
     lam_ref, gain_ref, mix_ref, q_hbm, k_hbm, v_hbm, up_hbm, dn_hbm, tok_hbm, ow_hbm,
-    out_hbm,
+    out_rows,
     q_ref, k_ref, v_ref, up_ref, dn_ref, tok_ref,
     ah, upf_ref, dnf_ref,
-    qb, kv, qm, run_max, run_sum, acc, att, ow, tokall, normed, hid, part, core_in, cross, cross_in, out_rows,
+    qb, kv, qm, run_max, run_sum, acc, att, ow, tokall, normed, hid, part, core_in, cross, cross_in,
     ex_send, ex_recv, top_recv, swap_send, tk_send, tk_recv, kv_send, kv_recv,
     w_send, own_send, y_send, w_recv, u_send, u_recv, a_send, a_recv, loc, own_att, put_sem, in_sem,
     c_send, first_recv, c_recv, x_send, x_recv,
@@ -386,12 +386,11 @@
                 from_core(k, z)
 
         token_own(1).start()
-        token_own(0).wait_recv()
-        token_half(0).start()
 
     def pass_tokens():
-        token_own(1).wait_recv()
-        token_half(1).start()
+        for k in (1, 0):
+            token_own(k).wait_recv()
+            token_half(k).start()
 
     @pl.when(jnp.logical_not(top))
     def _():
@@ -403,8 +402,8 @@
 
     @pl.when(helper)
     def _():
+        spread()
         lax.fori_loop(1, 2, diagonal, 0)
-        spread()
         for hh in range(2):
             tiles(1, z, hh)
 
@@ -422,11 +421,21 @@
         forward_now = jnp.logical_and(d == jnp.where(helper, 1, 2), jnp.logical_not(forwarded))
         pl.when(forward_now)(lambda: from_below(1, UPS))
 
+        @pl.when(jnp.logical_and(helper, d == 2))
+        def _():
+            pass_tokens()
+            from_above(1, DOWNS[:1])
+
+
+        def ahead():
+            from_above(1, DOWNS[1:])
+            from_below(2, UPS[:1])
+
         def slot(v, inner):
             u, hh = 1 - v // 2, lax.rem(v, 2)
             own_turn = jnp.logical_and(v == 2, helper)
             pl.when(jnp.logical_and(own_turn, d == 1))(lambda: from_above(1, UPS))
-            pl.when(jnp.logical_and(own_turn, d == 2))(pass_tokens)
+            pl.when(jnp.logical_and(helper, jnp.logical_and(v == 3, d == 2)))(ahead)
             tiles(u, j, hh)
 
             @pl.when(d == z)
@@ -440,7 +449,7 @@
         lax.fori_loop(jnp.where(helper, 0, 2), 4, slot, 0)
         pl.when(jnp.logical_and(d == 1, middle))(spread)
         pl.when(jnp.logical_and(d == 1, kv_rises))(lambda: from_above(1, UPS))
-        pl.when(d == 2)(lambda: from_above(1, DOWNS))
+        pl.when(jnp.logical_and(d == 2, kv_rises))(lambda: from_above(1, DOWNS))
         return carry
 
     lax.fori_loop(1, jnp.where(top, 1, z + 1), block, 0)
@@ -468,17 +477,19 @@
 
     @pl.when(z == 1)
     def _():
-        from_below(1, UPS)
+        pl.when(jnp.logical_not(forwarded))(lambda: from_below(1, UPS))
         late_down()
         from_above(1, DOWNS[:1])
-        pass_tokens()
         from_above(2, UPS)
         from_above(1, DOWNS[1:])
+        pass_tokens()
+        from_above(2, DOWNS)
 
     @pl.when(jnp.logical_and(z >= 2, has_up))
     def _():
         pl.when(jnp.logical_not(helper))(pass_tokens)
-        from_below(2, UPS)
+        pl.when(jnp.logical_not(helper))(lambda: from_below(2, UPS[:1]))
+        from_below(2, UPS[1:])
         pl.when(helper)(lambda: from_below(1, DOWNS[:1]))
 
     @pl.when(top)
@@ -560,19 +571,21 @@
             cross[j, hf] = (part[j, hf, where].astype(f32) + core_in[j, 1, hf].astype(f32)).astype(bf16)
             to_second(j, e, hf).start()
 
-    def multiply(i, hf):
-        for e in range(2):
-            j = 2 * i + e
-            product = jnp.dot(hid[hf], dnf_ref[j], preferred_element_type=f32).astype(bf16)
-            part[j, hf] = product.reshape(tp, half_piece, product.shape[1])
-        for e in range(2):
-            j = 2 * i + e
-            to_first(j, e, 1, hf).start()
-            to_first(j, e, 0, hf).start()
+    def multiply(i, hfs):
+        for hf in hfs:
+            for e in range(2):
+                j = 2 * i + e
+                product = jnp.dot(hid[hf], dnf_ref[j], preferred_element_type=f32).astype(bf16)
+                part[j, hf] = product.reshape(tp, half_piece, product.shape[1])
+            for e in range(2):
+                to_first(2 * i + e, e, 1, hf).start()
+        for hf in hfs:
+            for e in range(2):
+                to_first(2 * i + e, e, 0, hf).start()
 
     def arrivals(k):
         i = order(k)
-        pl.when(i - z >= 2)(lambda: from_above(i - z, DOWNS))
+        pl.when(i - z >= jnp.where(z == 1, 3, 2))(lambda: from_above(i - z, DOWNS))
         pl.when(z - i >= jnp.where(helper, 3, 2))(lambda: from_below(z - i, DOWNS))
         for m in DOWNS:
             pl.when(jnp.logical_not(jnp.logical_and(own_line, i == z)))(lambda: from_core(m, i))
@@ -582,7 +595,7 @@
 
     def early_pair(k, carry):
         arrivals(k)
-        multiply(order(k), 0)
+        multiply(order(k), (0,))
         return carry
 
     lax.fori_loop(0, ready, early_pair, 0)
@@ -592,7 +605,7 @@
 
     def second_pair(k, carry):
         relay(order(k), 0)
-        multiply(order(k), 1)
+        multiply(order(k), (1,))
         return carry
 
     lax.fori_loop(0, ready, second_pair, 0)
@@ -607,8 +620,7 @@
         final = k == steps - 1
         pl.when(jnp.logical_and(edge, final))(lambda: relay_both(k - 1))
         arrivals(k)
-        for hf in range(2):
-            multiply(order(k), hf)
+        multiply(order(k), (0, 1))
 
         @pl.when(k == ready)
         def _():
@@ -646,23 +658,8 @@
 
         lax.fori_loop(0, z + 1, sent, 0)
 
-    def line_sent(i, carry):
-        gone = jnp.logical_or(jnp.logical_and(i <= z, has_up), jnp.logical_and(i > z, has_down))
-        pl.when(gone)(lambda: drain(a_shard, w_send.at[2 * i + c]))
-        return carry
-
-    lax.fori_loop(0, steps, line_sent, 0)
-    drain(upf_ref, y_send.at[0])
-    pl.when(has_down)(lambda: drain(a_shard, own_send.at[0]))
-
     relay_both(steps - 1)
     cols = dn_ref.shape[1]
-    width = out_hbm.shape[1]
-
-    def put(i):
-        here = slice(i * (width // 2), (i + 1) * (width // 2))
-        return pltpu.make_async_copy(out_rows.at[:, here], out_hbm.at[:, here], put_sem.at[i])
-
     def close(js):
         for at, j in enumerate(js):
             mine_in = core_in.at[j, 0]
@@ -671,16 +668,20 @@
             here = slice(j * cols, (j + 1) * cols)
             both = part[j, :, b].astype(f32) + core_in[j, 0].astype(f32) + cross_in[j].astype(f32)
             out_rows[:, here] = (tokall[b, :, here].astype(f32) + both.reshape(piece, cols)).astype(bf16)
-            if (at + 1) % (n // 2) == 0:
-                put(j // (n // 2)).start()
 
     pl.when(z == 0)(lambda: close(tuple(range(n))))
     pl.when(z > 0)(lambda: close(tuple(range(n - 1, -1, -1))))
 
     drain(core_in, c_send.at[0])
     drain(cross, x_send.at[0])
-    for i in range(2):
-        put(i).wait()
+    def line_sent(i, carry):
+        gone = jnp.logical_or(jnp.logical_and(i <= z, has_up), jnp.logical_and(i > z, has_down))
+        pl.when(gone)(lambda: drain(a_shard, w_send.at[2 * i + c]))
+        return carry
+
+    lax.fori_loop(0, steps, line_sent, 0)
+    drain(upf_ref, y_send.at[0])
+    pl.when(has_down)(lambda: drain(a_shard, own_send.at[0]))
 
 
 def per_device(
@@ -695,9 +696,9 @@
     dma = pltpu.SemaphoreType.DMA
     return pl.pallas_call(
         functools.partial(layer_kernel, n, tp),
-        out_shape=jax.ShapeDtypeStruct(tokens.shape, bf16),
+        out_shape=pltpu.VMEM(tokens.shape, bf16),
         in_specs=[pl.BlockSpec(memory_space=pltpu.SMEM)] + [vmem] * 2 + [pl.BlockSpec(memory_space=pl.ANY)] * 7,
-        out_specs=pl.BlockSpec(memory_space=pl.ANY),
+        out_specs=pl.BlockSpec(memory_space=pltpu.VMEM),
         scratch_shapes=[
             pltpu.VMEM(queries.shape, bf16), pltpu.VMEM(keys.shape, bf16), pltpu.VMEM(values.shape, bf16),
             pltpu.VMEM(up_weight.shape, bf16), pltpu.VMEM(down_weight.shape, bf16), pltpu.VMEM(tokens.shape, bf16),
@@ -719,7 +720,6 @@
             pltpu.VMEM((n, 2, 2, piece // 2, cols), bf16),
             pltpu.VMEM((n, 2, piece // 2, cols), bf16),
             pltpu.VMEM((n, 2, piece // 2, cols), bf16),
-            pltpu.VMEM((piece, width), bf16),
             dma((3,)), dma((3,)), dma((2,)), dma((1,)), dma((4,)), dma((4,)),
             dma((n // 2,)), dma((n // 2, 2)),
             dma((n,)), dma((1,)), dma((1,)), dma((n, CHUNKS)), dma((2,)), dma((2,)),

time: 97.8 us -> 93.3 us (0.954)
  Pallas kernels: 95.6 us -> 92.3 us
  local copies, waits for them, and re-layouts: 1.88 us -> 0.8 us
    pallas_call x1, Pallas kernels: 95.6 us -> 92.3 us  [per_device(): pl.pallas_call(functools.partial(layer_kernel, n, tp), out_shape=pltpu.VM...]
    unnamed x1, local copies, waits for them, and re-layouts: 1.88 us -> 0.8 us
where the time goes in v4:
time: 93.3 us; the launch traced here: 93.1 us
  Pallas kernels  92.3 us (99%)
    pallas_call x1, Pallas kernels, per_device(): pl.pallas_call(functools.partial(layer_kernel, n, tp), out_shape=pltpu.VM...  92.3 us

profile of v4, /device:TPU:25, one launch (start us, length us, event | category | flops | bytes accessed | tf_op | source)
XLA Modules:
  0.0 93.1 jit_solution(3598622637542869462)
XLA Ops:
  0.0 92.3 %shard_map.100 = bf16[128,2048]{1,0:T(8,128)(2,1)S(1)} custom-call(f32[2]{0:T(128)} %lam_ref.1, f32[1,128]{1,0:T(1,128)} %bitcast.3, f32[1,2048]{1,0:T(1,128)} %bitcast.2, bf16[512,256]{1,0:T(8,128)(2,1)} %q_hbm.1, bf16[512,256]{1,0:T(8,128)(2,1)} %k_hbm.1, bf16[512,256]{1,0:T(8,128)(2,1)} %v_hbm.1, bf16[256,1024]{1,0:T(8,128)(2,1)} %up_hbm.1, ...), custom_call_target="tpu_custom_call" | custom-call | tf_op jit(solution)/shard_map/pallas_call | solution.py:697
  92.3 0.8 copy.12

commit v5 on v4

--- a/solution.py
+++ b/solution.py
@@ -22,8 +22,8 @@
     ah, upf_ref, dnf_ref,
     qb, kv, qm, run_max, run_sum, acc, att, ow, tokall, normed, hid, part, core_in, cross, cross_in,
     ex_send, ex_recv, top_recv, swap_send, tk_send, tk_recv, kv_send, kv_recv,
-    w_send, own_send, y_send, w_recv, u_send, u_recv, a_send, a_recv, loc, own_att, put_sem, in_sem,
-    c_send, first_recv, c_recv, x_send, x_recv,
+    w_send, own_send, y_send, w_recv, u_send, u_recv, a_send, a_recv, loc, own_att, in_sem,
+    c_send, first_recv, c_recv, x_send,
 ):
     s = lax.axis_index("sp")
     t = lax.axis_index("tp")
@@ -420,12 +420,7 @@
 
         forward_now = jnp.logical_and(d == jnp.where(helper, 1, 2), jnp.logical_not(forwarded))
         pl.when(forward_now)(lambda: from_below(1, UPS))
-
-        @pl.when(jnp.logical_and(helper, d == 2))
-        def _():
-            pass_tokens()
-            from_above(1, DOWNS[:1])
-
+        pl.when(jnp.logical_and(helper, d == 2))(pass_tokens)
 
         def ahead():
             from_above(1, DOWNS[1:])
@@ -435,6 +430,7 @@
             u, hh = 1 - v // 2, lax.rem(v, 2)
             own_turn = jnp.logical_and(v == 2, helper)
             pl.when(jnp.logical_and(own_turn, d == 1))(lambda: from_above(1, UPS))
+            pl.when(jnp.logical_and(own_turn, d == 2))(lambda: from_above(1, DOWNS[:1]))
             pl.when(jnp.logical_and(helper, jnp.logical_and(v == 3, d == 2)))(ahead)
             tiles(u, j, hh)
 
@@ -482,6 +478,7 @@
         from_above(1, DOWNS[:1])
         from_above(2, UPS)
         from_above(1, DOWNS[1:])
+        from_below(1, DOWNS)
         pass_tokens()
         from_above(2, DOWNS)
 
@@ -528,7 +525,7 @@
 
     lax.fori_loop(2, steps, later_ups, 0)
     pl.when(jnp.logical_and(z > 1, kv_rises))(late_down)
-    pl.when(jnp.logical_and(z >= 1, kv_rises))(lambda: from_below(1, DOWNS))
+    pl.when(jnp.logical_and(z > 1, kv_rises))(lambda: from_below(1, DOWNS))
 
     @pl.when(own_line)
     def _():
@@ -560,7 +557,7 @@
 
     def to_second(j, e, hf):
         return remote(
-            cross.at[j, hf], cross_in.at[j, hf], x_send.at[0], x_recv.at[j], first[1 - e][0]
+            cross.at[j, hf], cross_in.at[j, hf], x_send.at[0], first_recv.at[j], first[1 - e][0]
         )
 
     def relay(i, hf):
@@ -662,9 +659,8 @@
     cols = dn_ref.shape[1]
     def close(js):
         for at, j in enumerate(js):
-            mine_in = core_in.at[j, 0]
-            remote(mine_in, mine_in, c_send.at[0], first_recv.at[j], beside).wait_recv()
-            remote(cross_in.at[j], cross_in.at[j], x_send.at[0], x_recv.at[j], beside).wait_recv()
+            both_in = core_in.at[j]
+            remote(both_in, both_in, c_send.at[0], first_recv.at[j], beside).wait_recv()
             here = slice(j * cols, (j + 1) * cols)
             both = part[j, :, b].astype(f32) + core_in[j, 0].astype(f32) + cross_in[j].astype(f32)
             out_rows[:, here] = (tokall[b, :, here].astype(f32) + both.reshape(piece, cols)).astype(bf16)
@@ -723,8 +719,8 @@
             dma((3,)), dma((3,)), dma((2,)), dma((1,)), dma((4,)), dma((4,)),
             dma((n // 2,)), dma((n // 2, 2)),
             dma((n,)), dma((1,)), dma((1,)), dma((n, CHUNKS)), dma((2,)), dma((2,)),
-            dma((1,)), dma((1,)), dma((7,)), dma((2,)), dma((2,)), dma((6,)),
-            dma((1,)), dma((n,)), dma((n, 2)), dma((1,)), dma((n,)),
+            dma((1,)), dma((1,)), dma((7,)), dma((2,)), dma((6,)),
+            dma((1,)), dma((n,)), dma((n, 2)), dma((1,)),
         ],
         compiler_params=pltpu.CompilerParams(
             collective_id=0, has_side_effects=True, vmem_limit_bytes=60 * 1024 * 1024

time: 93.3 us -> 93.4 us (level)
  no operation moved by 1% of the time
where the time goes in v5:
time: 93.4 us; the launch traced here: 93.2 us
  Pallas kernels  92.4 us (99%)
    pallas_call x1, Pallas kernels, per_device(): pl.pallas_call(functools.partial(layer_kernel, n, tp), out_shape=pltpu.VM...  92.4 us

profile of v5, /device:TPU:25, one launch (start us, length us, event | category | flops | bytes accessed | tf_op | source)
XLA Modules:
  0.0 93.2 jit_solution(4134047616682927560)
XLA Ops:
  0.0 92.4 %shard_map.100 = bf16[128,2048]{1,0:T(8,128)(2,1)S(1)} custom-call(f32[2]{0:T(128)} %lam_ref.1, f32[1,128]{1,0:T(1,128)} %bitcast.3, f32[1,2048]{1,0:T(1,128)} %bitcast.2, bf16[512,256]{1,0:T(8,128)(2,1)} %q_hbm.1, bf16[512,256]{1,0:T(8,128)(2,1)} %k_hbm.1, bf16[512,256]{1,0:T(8,128)(2,1)} %v_hbm.1, bf16[256,1024]{1,0:T(8,128)(2,1)} %up_hbm.1, ...), custom_call_target="tpu_custom_call" | custom-call | tf_op jit(solution)/shard_map/pallas_call | solution.py:693
  92.4 0.8 copy.12
